TPU v7x, 256 devices: a 4x2x16 block of a 4x16x16 slice. The times are simulated.
256 devices in a mesh: grp: 2 (over y), sp: 64 (over z, x), tp: 2 (over core).
Axes of the slice: x: 4, y: 2, z: 16, core: 2. Of those that a mesh axis runs over, the one named last changes fastest.
The devices are a block of a 4x16x16 slice.
Arguments:
- layer_input: bfloat16 [4, 8192, 2048], P('grp', ('sp', 'tp')), parts along dimension 0, may hold values from -6 to 6
- norm_gain: float32 [2048], replicated, may hold values from 0.1 to 1.9
- in_weight: bfloat16 [2048, 1024], P(None, 'tp'), may hold values from -0.125 to 0.125
- gate_weight: bfloat16 [2048, 1024], P(None, 'tp'), may hold values from -0.125 to 0.125
- rate_real: float32 [64, 64], P('tp'), may hold values from -1 to 0
- rate_imag: float32 [64, 64], P('tp'), may hold values from -3 to 3
- log_step: float32 [64], P('tp'), may hold values from -8 to -2.5
- input_real: bfloat16 [64, 64, 16], P('tp'), may hold values from -4 to 4
- input_imag: bfloat16 [64, 64, 16], P('tp'), may hold values from -4 to 4
- output_real: bfloat16 [64, 16, 64], P('tp'), may hold values from -10 to 10
- output_imag: bfloat16 [64, 16, 64], P('tp'), may hold values from -10 to 10
- skip_weight: float32 [1024], P('tp'), may hold values from -20 to 20
- decay_offset: float32 [4, 8192, 64], P('grp', 'sp', 'tp'), parts along dimension 0, may hold values from -1.5 to 0
- channel_gain: float32 [1024], replicated, may hold values from 0.1 to 1.9
- out_weight: bfloat16 [1024, 2048], P('tp'), may hold values from -0.1875 to 0.1875
Outputs:
- layer_output: bfloat16 [4, 8192, 2048], P('grp', ('sp', 'tp')), parts along dimension 0
There are 2 independent parts, one for each index of `grp`. A program takes and returns all parts, laid end to end along the dimension named above; an argument that names none is the same for every part. Nothing has to cross between parts.
All inputs are finite; a program needn't handle non-finite values.
Results may differ from a plain program's by a relative error of at most 0.014.
Values may be sent and summed in bfloat16 or wider, within the bound.
A program may use at most 128 MiB of HBM per device.

v0:
```python
import functools
import math

import jax
import jax.numpy as jnp
from jax import lax
from jax.experimental import pallas as pl
from jax.experimental.pallas import tpu as pltpu
from jax.sharding import Mesh
from jax.sharding import PartitionSpec as P

SP = ("sp_0", "sp_1")
SP_TP = ("sp_0", "sp_1", "tp")
MESH = pl.DeviceIdType.MESH
F32 = jnp.float32
BF16 = jnp.bfloat16
EPS = 1e-06
LANES = 128
CHUNKS = 8


def dot(a, b):
    return jnp.dot(a, b, preferred_element_type=F32)


def dot_t(a, b):
    return lax.dot_general(a, b, (((1,), (1,)), ((), ())), preferred_element_type=F32)


def iota(shape, dim):
    return lax.broadcasted_iota(jnp.int32, shape, dim)


def one_hot(cond):
    return jnp.where(cond, 1.0, 0.0).astype(BF16)


def split(value):
    high = value.astype(BF16)
    rest = value - high.astype(F32)
    middle = rest.astype(BF16)
    low = (rest - middle.astype(F32)).astype(BF16)
    return high, middle, low


def exact_dot(value, table):
    high, middle, low = split(value)
    return dot(high, table) + dot(middle, table) + dot(low, table)


def cmul(a, b):
    return a[0] * b[0] - a[1] * b[1], a[0] * b[1] + a[1] * b[0]


def small_expm1(x):
    series = x * (1.0 + x * (1 / 2 + x * (1 / 6 + x * (1 / 24 + x * (1 / 120 + x * (1 / 720 + x / 5040))))))
    return jnp.where(x > -0.3, series, jnp.exp(x) - 1.0)


def scan_order(rows):
    steps = rows // CHUNKS
    at = iota((rows, rows), 0)
    return one_hot(iota((rows, rows), 1) == (at & (CHUNKS - 1)) * steps + (at >> 3))


def natural_order(rows):
    steps = rows // CHUNKS
    at = iota((rows, rows), 1)
    return one_hot(iota((rows, rows), 0) == (at & (CHUNKS - 1)) * steps + (at >> 3))


def project_kernel(
    x_hbm,
    gain_ref,
    in_hbm,
    gate_hbm,
    inputs_ref,
    gates_ref,
    tokens,
    in_w,
    gate_w,
    normed,
    raw_in,
    raw_gate,
    local_sem,
    send_sem,
    recv_sem,
):
    tp = lax.axis_index("tp")
    sequences, own, depth = x_hbm.shape
    width = in_w.shape[1]
    barrier = pltpu.get_barrier_semaphore()
    pl.semaphore_signal(barrier, inc=1, device_id={"tp": 1 - tp}, device_id_type=MESH)
    mine = pl.ds(pl.multiple_of(tp * own, own), own)
    copies = [
        pltpu.make_async_copy(x_hbm, tokens.at[:, mine, :], local_sem.at[0]),
        pltpu.make_async_copy(in_hbm, in_w, local_sem.at[1]),
        pltpu.make_async_copy(gate_hbm, gate_w, local_sem.at[2]),
    ]
    for copy in copies:
        copy.start()
    pl.semaphore_wait(barrier, 1)
    remote = pltpu.make_async_remote_copy(
        src_ref=x_hbm,
        dst_ref=tokens.at[:, mine, :],
        send_sem=send_sem,
        recv_sem=recv_sem,
        device_id={"tp": 1 - tp},
        device_id_type=MESH,
    )
    remote.start()

    def norm(side):
        per = own // 16

        @pl.loop(0, sequences * per)
        def _(i):
            s = i // per
            row = pl.multiple_of(side * own + (i % per) * 16, 16)
            wide = tokens[s, pl.ds(row, 16), :].astype(F32)
            scale = lax.rsqrt(jnp.mean(wide * wide, axis=-1, keepdims=True) + EPS)
            normed[pl.ds(pl.multiple_of(i * 16, 16), 16), :] = (wide * scale * gain_ref[...]).astype(BF16)

    def project(side, weight, out):
        rows = pl.ds(pl.multiple_of(side * own, own), own)

        @pl.loop(0, width // 256)
        def _(c):
            lanes = pl.ds(pl.multiple_of(c * 256, 256), 256)
            part = dot(normed[...], weight[:, lanes])
            out[:, rows, lanes] = part.reshape(sequences, own, 256).astype(BF16)

    copies[0].wait()
    norm(tp)
    copies[1].wait()
    project(tp, in_w, raw_in)
    copies[2].wait()
    project(tp, gate_w, raw_gate)
    remote.wait()
    norm(1 - tp)
    project(1 - tp, in_w, raw_in)
    project(1 - tp, gate_w, raw_gate)
    rows = sequences * 2 * own
    order = scan_order(rows)
    inputs_ref[...] = dot(order, raw_in[...].reshape(rows, width)).astype(BF16)
    gates_ref[...] = dot(order, raw_gate[...].reshape(rows, width)).astype(BF16)


def mixer_kernel(
    inputs_ref,
    gates_ref,
    rate_re_ref,
    rate_im_ref,
    log_step_ref,
    table_re_ref,
    table_im_ref,
    read_re_ref,
    read_im_ref,
    skip_ref,
    offset_ref,
    gain_ref,
    out_w_hbm,
    out_ref,
    out_w,
    mags,
    drive_re,
    drive_im,
    states_re,
    states_im,
    lift_re,
    lift_im,
    vec,
    ends,
    before,
    init,
    log_pack,
    log_x,
    log_row,
    log_z,
    sum_stage,
    sum_pack,
    sum_x,
    sum_row,
    sum_z,
    carry_pack,
    carry_x,
    lam_pack,
    act,
    act_in,
    w_sem,
    w_send,
    w_recv,
    lx_send,
    lx_recv,
    lz_send,
    lz_recv,
    sx_send,
    sx_recv,
    sz_send,
    sz_recv,
    cx_send,
    cx_recv,
    a_send,
    a_recv,
):
    nz, nx = lax.axis_size("sp_0"), lax.axis_size("sp_1")
    mz, mx, tp = lax.axis_index("sp_0"), lax.axis_index("sp_1"), lax.axis_index("tp")
    rows, width = inputs_ref.shape
    groups, states = rate_re_ref.shape
    modes = groups * states
    steps = rows // CHUNKS
    sequences, own, depth = out_ref.shape
    quarters = CHUNKS // sequences
    part = modes // nx
    blocks = part // LANES
    tile = sequences * blocks
    half = modes // 2

    log_z[...] = jnp.zeros_like(log_z)
    sum_z[...] = jnp.zeros_like(sum_z)
    barrier = pltpu.get_barrier_semaphore()
    for d in range(1, nx):
        pl.semaphore_signal(barrier, inc=1, device_id={"sp_1": lax.rem(mx + d, nx)}, device_id_type=MESH)
    for d in range(1, nz):
        pl.semaphore_signal(barrier, inc=1, device_id={"sp_0": lax.rem(mz + d, nz)}, device_id_type=MESH)
    pl.semaphore_signal(barrier, inc=1, device_id={"tp": 1 - tp}, device_id_type=MESH)
    own_w = pltpu.make_async_copy(out_w_hbm, out_w.at[tp], w_sem)
    own_w.start()

    def to_x(source, target, send, recv):
        made = []
        for d in range(1, nx):
            k = lax.rem(mx + d, nx)
            made.append(
                pltpu.make_async_remote_copy(
                    src_ref=source.at[k],
                    dst_ref=target.at[mx],
                    send_sem=send.at[d - 1],
                    recv_sem=recv.at[d - 1],
                    device_id={"sp_1": k},
                    device_id_type=MESH,
                )
            )
        return made

    def to_z(source, target, send, recv):
        made = []
        for d in range(1, nz):
            made.append(
                pltpu.make_async_remote_copy(
                    src_ref=source,
                    dst_ref=target.at[d - 1],
                    send_sem=send.at[d - 1],
                    recv_sem=recv.at[d - 1],
                    device_id={"sp_0": lax.rem(mz + d, nz)},
                    device_id_type=MESH,
                )
            )
        return made

    def start_z(made):
        for d, copy in enumerate(made, 1):
            pl.when(mz + d < nz)(copy.start)

    def recv_z(made):
        for d, copy in enumerate(made, 1):
            pl.when(d <= mz)(copy.wait_recv)

    def sent_z(made):
        for d, copy in enumerate(made, 1):
            pl.when(mz + d < nz)(copy.wait_send)

    spread_g = one_hot((iota((groups, modes), 1) >> 6) == iota((groups, modes), 0))
    spread_p = one_hot((iota((states, modes), 1) & (states - 1)) == iota((states, modes), 0))

    offsets = offset_ref[...]
    chunk_logs = exact_dot(jnp.sum(offsets.reshape(CHUNKS, steps, groups), axis=1), spread_g)
    vec[pl.ds(16, CHUNKS), :] = chunk_logs
    for s in range(sequences):
        total = jnp.sum(chunk_logs[s * quarters : (s + 1) * quarters], axis=0, keepdims=True)
        for k in range(nx):
            for b in range(blocks):
                lo = k * part + b * LANES
                row = s * blocks + b
                log_pack[k, row : row + 1, :] = total[:, lo : lo + LANES]

    on_group = (iota((groups, modes), 1) >> 6) == iota((groups, modes), 0)

    def flat(ref):
        return jnp.sum(jnp.where(on_group, exact_dot(ref[...], spread_p), 0.0), axis=0, keepdims=True)

    step = exact_dot(jnp.broadcast_to(jnp.exp(log_step_ref[...]), (8, groups)), spread_g)[0:1]
    rate_re, rate_im = flat(rate_re_ref), flat(rate_im_ref)
    real_step, angle = rate_re * step, rate_im * step
    size = jnp.exp(real_step)
    cosine, sine = jnp.cos(angle), jnp.sin(angle)
    half_sine = jnp.sin(0.5 * angle)
    top_re = small_expm1(real_step) * cosine - 2.0 * half_sine * half_sine
    top_im = size * sine
    inverse = 1.0 / (rate_re * rate_re + rate_im * rate_im)
    coef_re = (top_re * rate_re + top_im * rate_im) * inverse
    coef_im = (top_im * rate_re - top_re * rate_im) * inverse
    lam = (size * cosine, size * sine)
    power = lam
    for _ in range(int(math.log2(steps))):
        power = cmul(power, power)
    lam_chunk = power
    for _ in range(int(math.log2(quarters))):
        power = cmul(power, power)
    for i, value in enumerate((*lam, *lam_chunk, *power, coef_re, coef_im)):
        vec[i : i + 1, :] = value

    order = scan_order(rows)
    pieces = [dot(order, piece) for piece in split(jnp.exp(offsets))]
    spread_3 = one_hot((iota((3 * groups, modes), 1) >> 6) == (iota((3 * groups, modes), 0) & (groups - 1)))
    mags[...] = dot(jnp.concatenate(pieces, axis=1).astype(BF16), spread_3)

    channels = table_re_ref.shape[1]
    eye = one_hot(iota((channels, channels), 0) == iota((channels, channels), 1))
    hw = width // 2
    same = (iota((hw, half), 0) >> 4) == (iota((hw, half), 1) >> 6)
    for h in range(2):
        for table, drive in ((table_re_ref, drive_re), (table_im_ref, drive_im)):
            turned = dot_t(eye, table[h * half : (h + 1) * half, :])
            wide = jnp.where(same, jnp.concatenate([turned] * (hw // channels), axis=0), 0.0).astype(BF16)
            drive[:, h * half : (h + 1) * half] = dot(inputs_ref[:, h * hw : (h + 1) * hw], wide)

    pl.semaphore_wait(barrier, nx + nz - 1)
    log_sends = to_x(log_pack, log_x, lx_send, lx_recv)
    for copy in log_sends:
        copy.start()
    w_copy = pltpu.make_async_remote_copy(
        src_ref=out_w_hbm,
        dst_ref=out_w.at[tp],
        send_sem=w_send,
        recv_sem=w_recv,
        device_id={"tp": 1 - tp},
        device_id_type=MESH,
    )
    w_copy.start()
    log_x[pl.ds(mx, 1)] = log_pack[pl.ds(mx, 1)]

    span = 512

    def scan(first, keep):
        @pl.loop(0, modes // span)
        def _(c):
            lanes = pl.ds(pl.multiple_of(c * span, span), span)
            lr = jnp.broadcast_to(vec[0:1, lanes], (CHUNKS, span))
            li = jnp.broadcast_to(vec[1:2, lanes], (CHUNKS, span))
            if first is None:
                start = (jnp.zeros((CHUNKS, span), F32), jnp.zeros((CHUNKS, span), F32))
            else:
                start = (first[0, :, lanes], first[1, :, lanes])

            def body(t, now):
                re, im = now
                at = pl.ds(pl.multiple_of(t * 16, 16), 16)
                m, dr, di = mags[at, lanes], drive_re[at, lanes], drive_im[at, lanes]
                kept = []
                for u in range(2):
                    use = slice(u * CHUNKS, (u + 1) * CHUNKS)
                    ar, ai = m[use] * lr, m[use] * li
                    re, im = ar * re - ai * im + dr[use], ar * im + ai * re + di[use]
                    kept.append((re, im))
                if keep:
                    states_re[at, lanes] = jnp.concatenate([k[0] for k in kept], axis=0).astype(BF16)
                    states_im[at, lanes] = jnp.concatenate([k[1] for k in kept], axis=0).astype(BF16)
                return re, im

            re, im = lax.fori_loop(0, steps // 2, body, start)
            if not keep:
                ends[0, :, lanes] = re
                ends[1, :, lanes] = im

    scan(None, False)

    place = iota((CHUNKS, modes), 0) & (quarters - 1)
    grown = jnp.exp(vec[pl.ds(16, CHUNKS), :])
    a = (grown * vec[2:3, :], grown * vec[3:4, :])
    b = (ends[0], ends[1])
    d = 1
    while d < quarters:
        ok = place >= d
        a_old = tuple(pltpu.roll(v, d, axis=0) for v in a)
        b_old = tuple(pltpu.roll(v, d, axis=0) for v in b)
        add = cmul(a, b_old)
        new_a = cmul(a, a_old)
        b = tuple(jnp.where(ok, v + w, v) for v, w in zip(b, add))
        a = tuple(jnp.where(ok, w, v) for v, w in zip(a, new_a))
        d *= 2
    for i, (value, empty) in enumerate(((a[0], 1.0), (a[1], 0.0), (b[0], 0.0), (b[1], 0.0))):
        before[i] = jnp.where(place == 0, empty, pltpu.roll(value, 1, axis=0))
    for c in range(2):
        for s in range(sequences):
            last = (s + 1) * quarters - 1
            for k in range(nx):
                for blk in range(blocks):
                    lo = k * part + blk * LANES
                    row = c * tile + s * blocks + blk
                    sum_stage[k, row : row + 1, :] = b[c][last : last + 1, lo : lo + LANES]
    sum_pack[...] = sum_stage[...].astype(BF16)
    sum_sends = to_x(sum_pack, sum_x, sx_send, sx_recv)
    for copy in sum_sends:
        copy.start()
    sum_x[pl.ds(mx, 1)] = sum_pack[pl.ds(mx, 1)]

    for copy in log_sends:
        copy.wait()
    log_row[...] = jnp.sum(log_x[...], axis=0)
    log_z_sends = to_z(log_row, log_z, lz_send, lz_recv)
    start_z(log_z_sends)
    for c in range(2):
        for blk in range(blocks):
            lanes = pl.ds(pl.multiple_of(mx * part + blk * LANES, LANES), LANES)
            value = vec[4 + c : 5 + c, lanes]
            for s in range(sequences):
                row = s * blocks + blk
                lam_pack[c, row : row + 1, :] = value
    lam_dev = (lam_pack[0], lam_pack[1])
    lam_row = lam_dev
    for _ in range(int(math.log2(nx))):
        lam_row = cmul(lam_row, lam_row)

    def grow(logs, base):
        size = jnp.exp(logs)
        return size * base[0], size * base[1]

    def halves(value):
        wide = value.astype(F32)
        return wide[:tile], wide[tile:]

    def step_over(carry, trans, add):
        moved = cmul(carry, trans)
        return moved[0] + add[0], moved[1] + add[1]

    for copy in sum_sends:
        copy.wait()
    nothing = (jnp.zeros((tile, LANES), F32), jnp.zeros((tile, LANES), F32))
    total = nothing
    for k in range(nx):
        total = step_over(total, grow(log_x[k], lam_dev), halves(sum_x[k]))
    sum_row[...] = jnp.concatenate(total, axis=0).astype(BF16)
    sum_z_sends = to_z(sum_row, sum_z, sz_send, sz_recv)
    start_z(sum_z_sends)

    reads = (iota((hw, half), 0) >> 4) == (iota((hw, half), 1) >> 6)
    for h in range(2):
        use = slice(h * hw, (h + 1) * hw)
        wide_re = dot(read_re_ref[use, :], spread_p[:, :half])
        wide_im = dot(read_im_ref[use, :], spread_p[:, :half])
        kr, ki = vec[6:7, h * half : (h + 1) * half], vec[7:8, h * half : (h + 1) * half]
        lift_re[use, :] = jnp.where(reads, wide_re * kr - wide_im * ki, 0.0).astype(BF16)
        lift_im[use, :] = jnp.where(reads, -(wide_re * ki + wide_im * kr), 0.0).astype(BF16)

    recv_z(log_z_sends)
    recv_z(sum_z_sends)
    carry = nothing
    for d in range(nz - 1, 0, -1):
        new = step_over(carry, grow(log_z[d - 1], lam_row), halves(sum_z[d - 1]))
        carry = tuple(jnp.where(d <= mz, n, o) for n, o in zip(new, carry))
    for k in range(nx):
        carry_pack[k] = jnp.concatenate(carry, axis=0).astype(BF16)
        carry = step_over(carry, grow(log_x[k], lam_dev), halves(sum_x[k]))
    carry_sends = to_x(carry_pack, carry_x, cx_send, cx_recv)
    for copy in carry_sends:
        copy.start()
    carry_x[pl.ds(mx, 1)] = carry_pack[pl.ds(mx, 1)]
    for copy in carry_sends:
        copy.wait()
    upper = iota((CHUNKS, LANES), 0) < quarters
    for k in range(nx):
        got = carry_x[k].astype(F32)
        for blk in range(blocks):
            lo = k * part + blk * LANES
            lanes = slice(lo, lo + LANES)
            came = tuple(
                jnp.where(upper, got[c * tile + blk][None], got[c * tile + blocks + blk][None]) for c in range(2)
            )
            moved = cmul((before[0, :, lanes], before[1, :, lanes]), came)
            init[0, :, lanes] = before[2, :, lanes] + moved[0]
            init[1, :, lanes] = before[3, :, lanes] + moved[1]

    scan(init, True)

    parts = []
    for h in range(2):
        use = slice(h * hw, (h + 1) * hw)
        lanes = slice(h * half, (h + 1) * half)
        mixed = dot_t(states_re[:, lanes], lift_re[use, :]) + dot_t(states_im[:, lanes], lift_im[use, :])
        mixed = mixed + skip_ref[:, use] * inputs_ref[:, use].astype(F32)
        gelu = 0.5 * mixed * (1.0 + lax.erf(mixed * math.sqrt(0.5)))
        gated = gelu / (1.0 + jnp.exp(-gates_ref[:, use].astype(F32)))
        parts.append(gated.astype(BF16))
    back = natural_order(rows)
    for h in range(2):
        act[:, :, h * hw : (h + 1) * hw] = dot(back, parts[h]).astype(BF16).reshape(sequences, 2 * own, hw)
    theirs = pl.ds(pl.multiple_of((1 - tp) * own, own), own)
    mine = pl.ds(pl.multiple_of(tp * own, own), own)
    a_copy = pltpu.make_async_remote_copy(
        src_ref=act.at[:, theirs, :],
        dst_ref=act_in,
        send_sem=a_send,
        recv_sem=a_recv,
        device_id={"tp": 1 - tp},
        device_id_type=MESH,
    )
    a_copy.start()
    near = act[:, mine, :].astype(F32).reshape(sequences * own, width)
    near_square = jnp.sum(near * near, axis=-1, keepdims=True)
    own_w.wait()
    w_copy.wait()
    a_copy.wait()
    far = act_in[...].astype(F32).reshape(sequences * own, width)
    scale = lax.rsqrt((near_square + jnp.sum(far * far, axis=-1, keepdims=True)) * (0.5 / width) + EPS)
    gain_near = gain_ref[:, pl.ds(pl.multiple_of(tp * width, width), width)]
    gain_far = gain_ref[:, pl.ds(pl.multiple_of((1 - tp) * width, width), width)]
    near = (near * scale * gain_near).astype(BF16)
    far = (far * scale * gain_far).astype(BF16)

    for c in range(depth // 256):
        lanes = slice(c * 256, (c + 1) * 256)
        result = dot(near, out_w[tp, :, lanes]) + dot(far, out_w[1 - tp, :, lanes])
        out_ref[:, :, lanes] = result.astype(BF16).reshape(sequences, own, 256)

    sent_z(log_z_sends)
    sent_z(sum_z_sends)


def vmem():
    return pl.BlockSpec(memory_space=pltpu.VMEM)


def hbm():
    return pl.BlockSpec(memory_space=pl.ANY)


def shards(
    layer_input,
    norm_gain,
    in_weight,
    gate_weight,
    rate_real,
    rate_imag,
    log_step,
    input_real,
    input_imag,
    output_real,
    output_imag,
    skip_weight,
    decay_offset,
    channel_gain,
    out_weight,
):
    nz, nx = lax.axis_size("sp_0"), lax.axis_size("sp_1")
    sequences, own, depth = layer_input.shape
    width = in_weight.shape[1]
    groups, states = rate_real.shape
    channels = input_real.shape[2]
    modes = groups * states
    rows = sequences * 2 * own
    dma = pltpu.SemaphoreType.DMA
    inputs, gates = pl.pallas_call(
        project_kernel,
        name="project",
        out_shape=[jax.ShapeDtypeStruct((rows, width), BF16)] * 2,
        in_specs=[hbm(), vmem(), hbm(), hbm()],
        out_specs=[vmem(), vmem()],
        scratch_shapes=[
            pltpu.VMEM((sequences, 2 * own, depth), BF16),
            pltpu.VMEM((depth, width), BF16),
            pltpu.VMEM((depth, width), BF16),
            pltpu.VMEM((sequences * own, depth), BF16),
            pltpu.VMEM((sequences, 2 * own, width), BF16),
            pltpu.VMEM((sequences, 2 * own, width), BF16),
            dma((3,)),
            dma,
            dma,
        ],
        compiler_params=pltpu.CompilerParams(collective_id=0, has_side_effects=True),
    )(layer_input, norm_gain[None], in_weight, gate_weight)

    tile = sequences * (modes // nx // LANES)
    f32 = functools.partial(pltpu.VMEM, dtype=F32)
    b16 = functools.partial(pltpu.VMEM, dtype=BF16)
    return pl.pallas_call(
        mixer_kernel,
        name="mixer",
        out_shape=jax.ShapeDtypeStruct((sequences, own, depth), BF16),
        in_specs=[vmem()] * 12 + [hbm()],
        out_specs=vmem(),
        scratch_shapes=[
            b16((2, width, depth)),
            f32((rows, modes)),
            f32((rows, modes)),
            f32((rows, modes)),
            b16((rows, modes)),
            b16((rows, modes)),
            b16((width, modes // 2)),
            b16((width, modes // 2)),
            f32((24, modes)),
            f32((2, CHUNKS, modes)),
            f32((4, CHUNKS, modes)),
            f32((2, CHUNKS, modes)),
            f32((nx, tile, LANES)),
            f32((nx, tile, LANES)),
            f32((tile, LANES)),
            f32((nz - 1, tile, LANES)),
            f32((nx, 2 * tile, LANES)),
            b16((nx, 2 * tile, LANES)),
            b16((nx, 2 * tile, LANES)),
            b16((2 * tile, LANES)),
            b16((nz - 1, 2 * tile, LANES)),
            b16((nx, 2 * tile, LANES)),
            b16((nx, 2 * tile, LANES)),
            f32((2, tile, LANES)),
            b16((sequences, 2 * own, width)),
            b16((sequences, own, width)),
            dma,
            dma,
            dma,
            dma((nx - 1,)),
            dma((nx - 1,)),
            dma((nz - 1,)),
            dma((nz - 1,)),
            dma((nx - 1,)),
            dma((nx - 1,)),
            dma((nz - 1,)),
            dma((nz - 1,)),
            dma((nx - 1,)),
            dma((nx - 1,)),
            dma,
            dma,
        ],
        compiler_params=pltpu.CompilerParams(collective_id=1, has_side_effects=True),
    )(
        inputs,
        gates,
        rate_real,
        rate_imag,
        log_step[None],
        input_real.reshape(modes, channels),
        input_imag.reshape(modes, channels),
        output_real.reshape(width, states),
        output_imag.reshape(width, states),
        skip_weight[None],
        decay_offset.reshape(rows, groups),
        channel_gain[None],
        out_weight,
    )


def solution(mesh):
    torus = Mesh(
        mesh.devices.reshape(mesh.shape["grp"], 16, 4, mesh.shape["tp"]),
        ("grp", "sp_0", "sp_1", "tp"),
    )
    return build(torus)


def build(torus):
    in_specs = (
        P("grp", SP_TP, None),
        P(),
        P(None, "tp"),
        P(None, "tp"),
        P("tp", None),
        P("tp", None),
        P("tp"),
        P("tp", None, None),
        P("tp", None, None),
        P("tp", None, None),
        P("tp", None, None),
        P("tp"),
        P("grp", SP, "tp"),
        P(),
        P("tp", None),
    )
    out_specs = P("grp", SP_TP, None)
    return jax.shard_map(shards, mesh=torus, in_specs=in_specs, out_specs=out_specs, check_vma=False)
```

profile of v0, /device:TPU:33, one launch (start us, length us, event | category | flops | bytes accessed | tf_op | source)
XLA Modules:
  0.0 56.5 jit_solution(1181035738053364399)
XLA Ops:
  0.0 1.5 %copy.18 = f32[2,128,32]{2,1,0:T(8,128)} copy(f32[2,128,32]{1,2,0:T(8,128)} %param.27) | data formatting | bytes 65536 | tf_op args[12]
  1.5 1.9 %copy.16 = bf16[32,64,16]{2,1,0:T(8,128)(2,1)} copy(bf16[32,64,16]{1,2,0:T(8,128)(2,1)} %param.22) | data formatting | bytes 131072 | tf_op args[7]
  3.4 1.9 %copy.17 = bf16[32,64,16]{2,1,0:T(8,128)(2,1)} copy(bf16[32,64,16]{1,2,0:T(8,128)(2,1)} %param.23) | data formatting | bytes 131072 | tf_op args[8]
  5.3 26.7 %project.1 = (bf16[256,512]{1,0:T(8,128)(2,1)}, bf16[256,512]{1,0:T(8,128)(2,1)}) custom-call(bf16[2,64,2048]{2,1,0:T(8,128)(2,1)} %x_hbm.1, f32[1,2048]{1,0:T(1,128)} %bitcast.14, bf16[2048,512]{1,0:T(8,128)(2,1)} %in_hbm.1, bf16[2048,512]{1,0:T(8,128)(2,1)} %gate_hbm.1), custom_call_target="tpu_custom_call" | custom-call | tf_op jit(solution)/shard_map/project/pallas_call | solution.py:563
  32.1 22.6 %mixer.1 = bf16[2,64,2048]{2,1,0:T(8,128)(2,1)} custom-call(bf16[256,512]{1,0:T(8,128)(2,1)} %get-tuple-element.7.inputs_ref, bf16[256,512]{1,0:T(8,128)(2,1)} %get-tuple-element.8.gates_ref, f32[32,64]{1,0:T(8,128)} %rate_re_ref.1, f32[32,64]{1,0:T(8,128)} %rate_im_ref.1, f32[1,32]{1,0:T(1,128)} %bitcast.17, bf16[2048,16]{1,0:T(8,128)(2,1)} %bitcast.9, ...), custom_call_target="tpu_custom_call" | custom-call | tf_op jit(solution)/shard_map/mixer/pallas_call | solution.py:586
  54.7 1.9 %copy.20 = bf16[2,64,2048]{2,1,0:T(8,128)(2,1)} copy(bf16[2,64,2048]{2,1,0:T(8,128)(2,1)} %mixer.1) | data formatting | bytes 1048576
where the time goes:
time: 56.9 us; the launch traced here: 56.5 us
  Pallas kernels  49.3 us (87%)
  local copies, waits for them, and re-layouts  7.2 us (13%)
    pallas_call x1, Pallas kernels, shards(): pl.pallas_call(project_kernel, name='project', out_shape=[jax.ShapeDtypeS...  26.7 us
    pallas_call x1, Pallas kernels, shards(): pl.pallas_call(mixer_kernel, name='mixer', out_shape=jax.ShapeDtypeStruct...  22.6 us
    unnamed x4, local copies, waits for them, and re-layouts  7.2 us

commit v1 on v0

v1 whole, which is shorter than its diff:
```python
import functools
import math

import jax
import jax.numpy as jnp
from jax import lax
from jax.experimental import pallas as pl
from jax.experimental.pallas import tpu as pltpu
from jax.sharding import Mesh
from jax.sharding import PartitionSpec as P

SP = ("sp_0", "sp_1")
SP_TP = ("sp_0", "sp_1", "tp")
MESH = pl.DeviceIdType.MESH
F32 = jnp.float32
BF16 = jnp.bfloat16
EPS = 1e-06
LANES = 128
CHUNKS = 8


def dot(a, b):
    return jnp.dot(a, b, preferred_element_type=F32)


def dot_t(a, b):
    return lax.dot_general(a, b, (((1,), (1,)), ((), ())), preferred_element_type=F32)


def iota(shape, dim):
    return lax.broadcasted_iota(jnp.int32, shape, dim)


def one_hot(cond):
    return jnp.where(cond, 1.0, 0.0).astype(BF16)


def split(value):
    high = value.astype(BF16)
    rest = value - high.astype(F32)
    middle = rest.astype(BF16)
    low = (rest - middle.astype(F32)).astype(BF16)
    return high, middle, low


def exact_dot(value, table):
    high, middle, low = split(value)
    return dot(high, table) + dot(middle, table) + dot(low, table)


def cmul(a, b):
    return a[0] * b[0] - a[1] * b[1], a[0] * b[1] + a[1] * b[0]


def small_expm1(x):
    series = x * (1.0 + x * (1 / 2 + x * (1 / 6 + x * (1 / 24 + x * (1 / 120 + x * (1 / 720 + x / 5040))))))
    return jnp.where(x > -0.3, series, jnp.exp(x) - 1.0)


def scan_order(rows):
    steps = rows // CHUNKS
    at = iota((rows, rows), 0)
    return one_hot(iota((rows, rows), 1) == (at & (CHUNKS - 1)) * steps + (at >> 3))


def natural_order(rows):
    steps = rows // CHUNKS
    at = iota((rows, rows), 1)
    return one_hot(iota((rows, rows), 0) == (at & (CHUNKS - 1)) * steps + (at >> 3))


def small_sine(x):
    q = x * x
    return x * (1.0 + q * (-1 / 6 + q * (1 / 120 + q * (-1 / 5040 + q * (1 / 362880 - q / 39916800)))))


def small_cosine(x):
    q = x * x
    return 1.0 + q * (-1 / 2 + q * (1 / 24 + q * (-1 / 720 + q * (1 / 40320 + q * (-1 / 3628800 + q / 479001600)))))


def mixer_kernel(
    x_hbm,
    in_w_hbm,
    gate_w_hbm,
    out_w_hbm,
    norm_gain_hbm,
    rate_re_hbm,
    rate_im_hbm,
    log_step_hbm,
    table_re_hbm,
    table_im_hbm,
    read_re_hbm,
    read_im_hbm,
    skip_hbm,
    offset_hbm,
    gain_hbm,
    out_ref,
    tokens,
    in_w,
    gate_w,
    out_w,
    norm_gain_ref,
    rate_re_ref,
    rate_im_ref,
    log_step_ref,
    table_re_ref,
    table_im_ref,
    read_re_ref,
    read_im_ref,
    skip_ref,
    offset_ref,
    gain_ref,
    normed,
    raw_in,
    raw_gate,
    inputs,
    opened,
    mags,
    wide_re,
    wide_im,
    drive_re,
    drive_im,
    states_re,
    states_im,
    lift_re,
    lift_im,
    vec,
    ends,
    before,
    init,
    log_pack,
    log_x,
    log_row,
    log_z,
    sum_stage,
    sum_pack,
    sum_x,
    sum_row,
    sum_z,
    carry_pack,
    carry_x,
    lam_pack,
    act,
    act_in,
    near_sum,
    load_sem,
    x_send,
    x_recv,
    w_send,
    w_recv,
    lx_send,
    lx_recv,
    lz_send,
    lz_recv,
    sx_send,
    sx_recv,
    sz_send,
    sz_recv,
    cx_send,
    cx_recv,
    a_send,
    a_recv,
):
    nz, nx = lax.axis_size("sp_0"), lax.axis_size("sp_1")
    mz, mx, tp = lax.axis_index("sp_0"), lax.axis_index("sp_1"), lax.axis_index("tp")
    sequences, own, depth = x_hbm.shape
    width = in_w_hbm.shape[1]
    rows = sequences * 2 * own
    groups, states = rate_re_hbm.shape
    channels = width // groups
    modes = groups * states
    steps = rows // CHUNKS
    quarters = CHUNKS // sequences
    part = modes // nx
    blocks = part // LANES
    tile = sequences * blocks
    half = modes // 2
    hw = width // 2
    mine = pl.ds(pl.multiple_of(tp * own, own), own)
    theirs = pl.ds(pl.multiple_of((1 - tp) * own, own), own)
    partner = {"tp": 1 - tp}

    loads = [
        pltpu.make_async_copy(source, target, load_sem.at[i])
        for i, (source, target) in enumerate(
            (
                (x_hbm, tokens.at[:, mine, :]),
                (offset_hbm, offset_ref),
                (rate_re_hbm, rate_re_ref),
                (rate_im_hbm, rate_im_ref),
                (log_step_hbm, log_step_ref),
                (norm_gain_hbm, norm_gain_ref),
                (table_re_hbm, table_re_ref),
                (table_im_hbm, table_im_ref),
                (in_w_hbm, in_w),
                (gate_w_hbm, gate_w),
                (read_re_hbm, read_re_ref),
                (read_im_hbm, read_im_ref),
                (skip_hbm, skip_ref),
                (gain_hbm, gain_ref),
                (out_w_hbm, out_w.at[tp]),
            )
        )
    ]
    for copy in loads:
        copy.start()

    log_z[...] = jnp.zeros_like(log_z)
    sum_z[...] = jnp.zeros_like(sum_z)
    barrier = pltpu.get_barrier_semaphore()
    pl.semaphore_signal(barrier, inc=1, device_id=partner, device_id_type=MESH)
    for d in range(1, nx):
        pl.semaphore_signal(barrier, inc=1, device_id={"sp_1": lax.rem(mx + d, nx)}, device_id_type=MESH)
    far_first = sorted(range(1, nz), key=lambda d: -min(d, nz - d))
    for d in far_first:
        pl.semaphore_signal(barrier, inc=1, device_id={"sp_0": lax.rem(mz + d, nz)}, device_id_type=MESH)

    def remote(source, target, send, recv, device):
        return pltpu.make_async_remote_copy(
            src_ref=source, dst_ref=target, send_sem=send, recv_sem=recv, device_id=device, device_id_type=MESH
        )

    def to_x(source, target, send, recv):
        made = []
        for d in range(1, nx):
            k = lax.rem(mx + d, nx)
            made.append(remote(source.at[k], target.at[mx], send.at[d - 1], recv.at[d - 1], {"sp_1": k}))
        return made

    def to_z(source, target, send, recv):
        return {
            d: remote(source, target.at[d - 1], send.at[d - 1], recv.at[d - 1], {"sp_0": lax.rem(mz + d, nz)})
            for d in far_first
        }

    def start_z(made):
        for d, copy in made.items():
            pl.when(mz + d < nz)(copy.start)

    def recv_z(made):
        for d, copy in made.items():
            pl.when(d <= mz)(copy.wait_recv)

    def sent_z(made):
        for d, copy in made.items():
            pl.when(mz + d < nz)(copy.wait_send)

    for copy in loads[1:6]:
        copy.wait()
    spread_g = one_hot((iota((groups, modes), 1) >> 6) == iota((groups, modes), 0))
    spread_p = one_hot((iota((states, modes), 1) & (states - 1)) == iota((states, modes), 0))
    offsets = jnp.concatenate([offset_ref[s].T for s in range(sequences)], axis=0)
    sums = jnp.sum(offsets.reshape(CHUNKS, steps, groups), axis=1)
    step_size = jnp.broadcast_to(jnp.exp(log_step_ref[...]), (8, groups))
    spread = exact_dot(jnp.concatenate([sums, step_size], axis=0), spread_g)
    chunk_logs, step = spread[:CHUNKS], spread[CHUNKS : CHUNKS + 1]
    vec[pl.ds(16, CHUNKS), :] = chunk_logs
    for s in range(sequences):
        total = jnp.sum(chunk_logs[s * quarters : (s + 1) * quarters], axis=0, keepdims=True)
        for k in range(nx):
            for b in range(blocks):
                lo = k * part + b * LANES
                row = s * blocks + b
                log_pack[k, row : row + 1, :] = total[:, lo : lo + LANES]

    pl.semaphore_wait(barrier, nx + nz - 1)
    x_copy = remote(x_hbm, tokens.at[:, mine, :], x_send, x_recv, partner)
    x_copy.start()
    log_sends = to_x(log_pack, log_x, lx_send, lx_recv)
    for copy in log_sends:
        copy.start()
    log_x[pl.ds(mx, 1)] = log_pack[pl.ds(mx, 1)]

    def norm(side):
        per = own // 16

        @pl.loop(0, sequences * per)
        def _(i):
            s = i // per
            row = pl.multiple_of(side * own + (i % per) * 16, 16)
            wide = tokens[s, pl.ds(row, 16), :].astype(F32)
            scale = lax.rsqrt(jnp.mean(wide * wide, axis=-1, keepdims=True) + EPS)
            at = pl.ds(pl.multiple_of(i * 16, 16), 16)
            normed[side, at, :] = (wide * scale * norm_gain_ref[...]).astype(BF16)

    def project(side, weight, out):
        @pl.loop(0, width // 256)
        def _(c):
            lanes = pl.ds(pl.multiple_of(c * 256, 256), 256)
            product = dot(normed[side], weight[:, lanes])
            at = pl.ds(pl.multiple_of(side * own, own), own)
            out[:, at, lanes] = product.reshape(sequences, own, 256).astype(BF16)

    loads[0].wait()
    norm(tp)
    loads[8].wait()
    project(tp, in_w, raw_in)

    on_group = (iota((groups, modes), 1) >> 6) == iota((groups, modes), 0)
    rates = exact_dot(jnp.concatenate([rate_re_ref[...], rate_im_ref[...]], axis=0), spread_p)
    rate_re = jnp.sum(jnp.where(on_group, rates[:groups], 0.0), axis=0, keepdims=True)
    rate_im = jnp.sum(jnp.where(on_group, rates[groups:], 0.0), axis=0, keepdims=True)
    real_step, angle = rate_re * step, rate_im * step
    size = jnp.exp(real_step)
    cosine, sine = small_cosine(angle), small_sine(angle)
    half_sine = small_sine(0.5 * angle)
    top_re = small_expm1(real_step) * cosine - 2.0 * half_sine * half_sine
    top_im = size * sine
    inverse = 1.0 / (rate_re * rate_re + rate_im * rate_im)
    coef_re = (top_re * rate_re + top_im * rate_im) * inverse
    coef_im = (top_im * rate_re - top_re * rate_im) * inverse
    lam = (size * cosine, size * sine)
    power = lam
    for _ in range(int(math.log2(steps))):
        power = cmul(power, power)
    lam_chunk = power
    for _ in range(int(math.log2(quarters))):
        power = cmul(power, power)
    for i, value in enumerate((*lam, *lam_chunk, *power, coef_re, coef_im)):
        vec[i : i + 1, :] = value

    order = scan_order(rows)
    pieces = [dot(order, piece) for piece in split(jnp.exp(offsets))]
    spread_3 = one_hot((iota((3 * groups, modes), 1) >> 6) == (iota((3 * groups, modes), 0) & (groups - 1)))
    mags[...] = dot(jnp.concatenate(pieces, axis=1).astype(BF16), spread_3)

    per_tile = LANES // states

    def doubled(value):
        return jnp.concatenate([value.astype(F32)] * per_tile, axis=1)

    on_lane = iota((channels, LANES), 1) // states

    def block_diagonal(target, value):
        target[...] = jnp.zeros_like(target)
        for g in range(groups):
            at = slice(g * channels, (g + 1) * channels)
            lo = (g % (groups // 2)) // per_tile * LANES
            kept = jnp.where(on_lane == g % per_tile, value(g, at), 0.0)
            target[at, lo : lo + LANES] = kept.astype(BF16)

    for copy in loads[6:8]:
        copy.wait()
    two_re, two_im = doubled(table_re_ref[...]), doubled(table_im_ref[...])
    block_diagonal(wide_re, lambda g, at: two_re[at])
    block_diagonal(wide_im, lambda g, at: two_im[at])

    x_copy.wait()
    norm(1 - tp)
    project(1 - tp, in_w, raw_in)
    inputs[...] = dot(order, raw_in[...].reshape(rows, width)).astype(BF16)

    for h in range(2):
        use, lanes = slice(h * hw, (h + 1) * hw), slice(h * half, (h + 1) * half)
        drive_re[:, lanes] = dot(inputs[:, use], wide_re[use, :])
        drive_im[:, lanes] = dot(inputs[:, use], wide_im[use, :])

    span = 512

    def scan(first, keep):
        @pl.loop(0, modes // span)
        def _(c):
            lanes = pl.ds(pl.multiple_of(c * span, span), span)
            lr = jnp.broadcast_to(vec[0:1, lanes], (CHUNKS, span))
            li = jnp.broadcast_to(vec[1:2, lanes], (CHUNKS, span))
            if first is None:
                start = (jnp.zeros((CHUNKS, span), F32), jnp.zeros((CHUNKS, span), F32))
            else:
                start = (first[0, :, lanes], first[1, :, lanes])

            def body(t, now):
                re, im = now
                at = pl.ds(pl.multiple_of(t * 16, 16), 16)
                m, dr, di = mags[at, lanes], drive_re[at, lanes], drive_im[at, lanes]
                kept = []
                for u in range(2):
                    use = slice(u * CHUNKS, (u + 1) * CHUNKS)
                    ar, ai = m[use] * lr, m[use] * li
                    re, im = ar * re - ai * im + dr[use], ar * im + ai * re + di[use]
                    kept.append((re, im))
                if keep:
                    states_re[at, lanes] = jnp.concatenate([k[0] for k in kept], axis=0).astype(BF16)
                    states_im[at, lanes] = jnp.concatenate([k[1] for k in kept], axis=0).astype(BF16)
                return re, im

            re, im = lax.fori_loop(0, steps // 2, body, start)
            if not keep:
                ends[0, :, lanes] = re
                ends[1, :, lanes] = im

    scan(None, False)

    place = iota((CHUNKS, modes), 0) & (quarters - 1)
    grown = jnp.exp(vec[pl.ds(16, CHUNKS), :])
    a = (grown * vec[2:3, :], grown * vec[3:4, :])
    b = (ends[0], ends[1])
    d = 1
    while d < quarters:
        ok = place >= d
        a_old = tuple(pltpu.roll(v, d, axis=0) for v in a)
        b_old = tuple(pltpu.roll(v, d, axis=0) for v in b)
        add = cmul(a, b_old)
        new_a = cmul(a, a_old)
        b = tuple(jnp.where(ok, v + w, v) for v, w in zip(b, add))
        a = tuple(jnp.where(ok, w, v) for v, w in zip(a, new_a))
        d *= 2
    for c in range(2):
        for s in range(sequences):
            last = (s + 1) * quarters - 1
            for k in range(nx):
                for blk in range(blocks):
                    lo = k * part + blk * LANES
                    row = c * tile + s * blocks + blk
                    sum_stage[k, row : row + 1, :] = b[c][last : last + 1, lo : lo + LANES]
    sum_pack[...] = sum_stage[...].astype(BF16)
    for i, (value, empty) in enumerate(((a[0], 1.0), (a[1], 0.0), (b[0], 0.0), (b[1], 0.0))):
        before[i] = jnp.where(place == 0, empty, pltpu.roll(value, 1, axis=0))
    sum_sends = to_x(sum_pack, sum_x, sx_send, sx_recv)
    for copy in sum_sends:
        copy.start()
    sum_x[pl.ds(mx, 1)] = sum_pack[pl.ds(mx, 1)]

    for copy in log_sends:
        copy.wait()
    log_row[...] = jnp.sum(log_x[...], axis=0)
    log_z_sends = to_z(log_row, log_z, lz_send, lz_recv)
    start_z(log_z_sends)
    for c in range(2):
        for blk in range(blocks):
            lanes = pl.ds(pl.multiple_of(mx * part + blk * LANES, LANES), LANES)
            value = vec[4 + c : 5 + c, lanes]
            for s in range(sequences):
                row = s * blocks + blk
                lam_pack[c, row : row + 1, :] = value
    lam_dev = (lam_pack[0], lam_pack[1])
    one = (jnp.ones((tile, LANES), F32), jnp.zeros((tile, LANES), F32))
    lam_pow = [one]
    for _ in range(nx):
        lam_pow.append(cmul(lam_pow[-1], lam_dev))

    def grow(logs, base):
        size = jnp.exp(logs)
        return size * base[0], size * base[1]

    def halves(value):
        wide = value.astype(F32)
        return wide[:tile], wide[tile:]

    def plus(u, v):
        return u[0] + v[0], u[1] + v[1]

    logs = [log_x[k] for k in range(nx)]
    to_end, to_start = [None] * nx, [None] * nx
    gone = jnp.zeros((tile, LANES), F32)
    for k in range(nx - 1, -1, -1):
        to_end[k] = grow(gone, lam_pow[nx - 1 - k])
        gone = gone + logs[k]
    gone = jnp.zeros((tile, LANES), F32)
    for k in range(nx):
        to_start[k] = grow(gone, lam_pow[k])
        gone = gone + logs[k]

    loads[9].wait()
    project(tp, gate_w, raw_gate)

    for copy in sum_sends:
        copy.wait()
    came = [halves(sum_x[k]) for k in range(nx)]
    total = cmul(to_end[0], came[0])
    for k in range(1, nx):
        total = plus(total, cmul(to_end[k], came[k]))
    sum_row[...] = jnp.concatenate(total, axis=0).astype(BF16)
    sum_z_sends = to_z(sum_row, sum_z, sz_send, sz_recv)
    start_z(sum_z_sends)
    w_copy = remote(out_w_hbm, out_w.at[tp], w_send, w_recv, partner)
    w_copy.start()

    project(1 - tp, gate_w, raw_gate)
    gates = dot(scan_order(rows), raw_gate[...].reshape(rows, width))
    opened[...] = 1.0 / (1.0 + jnp.exp(-gates))

    for copy in loads[10:14]:
        copy.wait()
    two_re, two_im = doubled(read_re_ref[...]), doubled(read_im_ref[...])

    def coef(g):
        lo = g // per_tile * LANES
        return vec[6:7, lo : lo + LANES], vec[7:8, lo : lo + LANES]

    def lifted_re(g, at):
        kr, ki = coef(g)
        return two_re[at] * kr - two_im[at] * ki

    def lifted_im(g, at):
        kr, ki = coef(g)
        return -(two_re[at] * ki + two_im[at] * kr)

    block_diagonal(lift_re, lifted_re)
    block_diagonal(lift_im, lifted_im)

    inside = [None] * nx
    inside[0] = (jnp.zeros((tile, LANES), F32), jnp.zeros((tile, LANES), F32))
    for k in range(1, nx):
        inside[k] = plus(cmul(inside[k - 1], grow(logs[k - 1], lam_dev)), came[k - 1])
    recv_z(log_z_sends)
    weights = {}
    gone, power = jnp.zeros((tile, LANES), F32), one
    for d in range(1, nz):
        weights[d] = grow(gone, power)
        gone = gone + log_z[d - 1]
        power = cmul(power, lam_pow[nx])

    recv_z(sum_z_sends)
    carry = inside[0]
    for d in range(1, nz):
        carry = plus(carry, cmul(weights[d], halves(sum_z[d - 1])))
    for k in range(nx):
        carry_pack[k] = jnp.concatenate(plus(cmul(carry, to_start[k]), inside[k]), axis=0).astype(BF16)
    carry_sends = to_x(carry_pack, carry_x, cx_send, cx_recv)
    for copy in carry_sends:
        copy.start()
    carry_x[pl.ds(mx, 1)] = carry_pack[pl.ds(mx, 1)]
    for copy in carry_sends:
        copy.wait()
    upper = iota((CHUNKS, LANES), 0) < quarters
    for k in range(nx):
        got = carry_x[k].astype(F32)
        for blk in range(blocks):
            lo = k * part + blk * LANES
            lanes = slice(lo, lo + LANES)
            into = tuple(
                jnp.where(upper, got[c * tile + blk][None], got[c * tile + blocks + blk][None]) for c in range(2)
            )
            moved = cmul((before[0, :, lanes], before[1, :, lanes]), into)
            init[0, :, lanes] = before[2, :, lanes] + moved[0]
            init[1, :, lanes] = before[3, :, lanes] + moved[1]

    scan(init, True)

    parts = []
    for h in range(2):
        use = slice(h * hw, (h + 1) * hw)
        lanes = slice(h * half, (h + 1) * half)
        mixed = dot_t(states_re[:, lanes], lift_re[use, :]) + dot_t(states_im[:, lanes], lift_im[use, :])
        mixed = mixed + skip_ref[:, use] * inputs[:, use].astype(F32)
        gelu = 0.5 * mixed * (1.0 + lax.erf(mixed * math.sqrt(0.5)))
        parts.append((gelu * opened[:, use]).astype(BF16))
    back = natural_order(rows)
    for h in range(2):
        act[:, :, h * hw : (h + 1) * hw] = dot(back, parts[h]).astype(BF16).reshape(sequences, 2 * own, hw)
    a_copy = remote(act.at[:, theirs, :], act_in, a_send, a_recv, partner)
    a_copy.start()
    near = act[:, mine, :].astype(F32).reshape(sequences * own, width)
    near_square = jnp.sum(near * near, axis=-1, keepdims=True)
    near = (near * gain_ref[:, pl.ds(pl.multiple_of(tp * width, width), width)]).astype(BF16)
    loads[14].wait()
    for c in range(depth // 256):
        lanes = slice(c * 256, (c + 1) * 256)
        near_sum[:, lanes] = dot(near, out_w[tp, :, lanes])
    w_copy.wait()
    a_copy.wait()
    far = act_in[...].astype(F32).reshape(sequences * own, width)
    scale = lax.rsqrt((near_square + jnp.sum(far * far, axis=-1, keepdims=True)) * (0.5 / width) + EPS)
    far = (far * gain_ref[:, pl.ds(pl.multiple_of((1 - tp) * width, width), width)]).astype(BF16)
    for c in range(depth // 256):
        lanes = slice(c * 256, (c + 1) * 256)
        result = (near_sum[:, lanes] + dot(far, out_w[1 - tp, :, lanes])) * scale
        out_ref[:, :, lanes] = result.astype(BF16).reshape(sequences, own, 256)

    sent_z(log_z_sends)
    sent_z(sum_z_sends)


def vmem():
    return pl.BlockSpec(memory_space=pltpu.VMEM)


def hbm():
    return pl.BlockSpec(memory_space=pl.ANY)


def shards(
    layer_input,
    norm_gain,
    in_weight,
    gate_weight,
    rate_real,
    rate_imag,
    log_step,
    input_real,
    input_imag,
    output_real,
    output_imag,
    skip_weight,
    decay_offset,
    channel_gain,
    out_weight,
):
    nz, nx = lax.axis_size("sp_0"), lax.axis_size("sp_1")
    sequences, own, depth = layer_input.shape
    width = in_weight.shape[1]
    groups, states = rate_real.shape
    modes = groups * states
    rows = sequences * 2 * own
    dma = pltpu.SemaphoreType.DMA
    tile = sequences * (modes // nx // LANES)
    f32 = functools.partial(pltpu.VMEM, dtype=F32)
    b16 = functools.partial(pltpu.VMEM, dtype=BF16)
    return pl.pallas_call(
        mixer_kernel,
        name="mixer",
        out_shape=jax.ShapeDtypeStruct((sequences, own, depth), BF16),
        in_specs=[hbm()] * 15,
        out_specs=vmem(),
        scratch_shapes=[
            b16((sequences, 2 * own, depth)),
            b16((depth, width)),
            b16((depth, width)),
            b16((2, width, depth)),
            f32((1, depth)),
            f32((groups, states)),
            f32((groups, states)),
            f32((1, groups)),
            b16((width, states)),
            b16((width, states)),
            b16((width, states)),
            b16((width, states)),
            f32((1, width)),
            f32((sequences, groups, 2 * own)),
            f32((1, 2 * width)),
            b16((2, sequences * own, depth)),
            b16((sequences, 2 * own, width)),
            b16((sequences, 2 * own, width)),
            b16((rows, width)),
            f32((rows, width)),
            f32((rows, modes)),
            b16((width, modes // 2)),
            b16((width, modes // 2)),
            f32((rows, modes)),
            f32((rows, modes)),
            b16((rows, modes)),
            b16((rows, modes)),
            b16((width, modes // 2)),
            b16((width, modes // 2)),
            f32((24, modes)),
            f32((2, CHUNKS, modes)),
            f32((4, CHUNKS, modes)),
            f32((2, CHUNKS, modes)),
            f32((nx, tile, LANES)),
            f32((nx, tile, LANES)),
            f32((tile, LANES)),
            f32((nz - 1, tile, LANES)),
            f32((nx, 2 * tile, LANES)),
            b16((nx, 2 * tile, LANES)),
            b16((nx, 2 * tile, LANES)),
            b16((2 * tile, LANES)),
            b16((nz - 1, 2 * tile, LANES)),
            b16((nx, 2 * tile, LANES)),
            b16((nx, 2 * tile, LANES)),
            f32((2, tile, LANES)),
            b16((sequences, 2 * own, width)),
            b16((sequences, own, width)),
            f32((sequences * own, depth)),
            dma((15,)),
            dma,
            dma,
            dma,
            dma,
            dma((nx - 1,)),
            dma((nx - 1,)),
            dma((nz - 1,)),
            dma((nz - 1,)),
            dma((nx - 1,)),
            dma((nx - 1,)),
            dma((nz - 1,)),
            dma((nz - 1,)),
            dma((nx - 1,)),
            dma((nx - 1,)),
            dma,
            dma,
        ],
        compiler_params=pltpu.CompilerParams(collective_id=0, has_side_effects=True),
    )(
        layer_input,
        in_weight,
        gate_weight,
        out_weight,
        norm_gain[None],
        rate_real,
        rate_imag,
        log_step[None],
        jnp.swapaxes(input_real, 1, 2).reshape(width, states),
        jnp.swapaxes(input_imag, 1, 2).reshape(width, states),
        output_real.reshape(width, states),
        output_imag.reshape(width, states),
        skip_weight[None],
        jnp.swapaxes(decay_offset, 1, 2),
        channel_gain[None],
    )


def solution(mesh):
    torus = Mesh(
        mesh.devices.reshape(mesh.shape["grp"], 16, 4, mesh.shape["tp"]),
        ("grp", "sp_0", "sp_1", "tp"),
    )
    return build(torus)


def build(torus):
    in_specs = (
        P("grp", SP_TP, None),
        P(),
        P(None, "tp"),
        P(None, "tp"),
        P("tp", None),
        P("tp", None),
        P("tp"),
        P("tp", None, None),
        P("tp", None, None),
        P("tp", None, None),
        P("tp", None, None),
        P("tp"),
        P("grp", SP, "tp"),
        P(),
        P("tp", None),
    )
    out_specs = P("grp", SP_TP, None)
    return jax.shard_map(shards, mesh=torus, in_specs=in_specs, out_specs=out_specs, check_vma=False)
```

time: 56.9 us -> 47.9 us (0.84)
  local copies, waits for them, and re-layouts: 7.2 us -> 1.88 us
  Pallas kernels: 49.3 us -> 45.9 us
    pallas_call x1 -> x0, Pallas kernels: 26.7 us -> none  [shards(): pl.pallas_call(project_kernel, name='project', out_shape=[jax.ShapeDtypeS...]
    pallas_call x1, Pallas kernels: 22.6 us -> 45.9 us  [shards(): pl.pallas_call(mixer_kernel, name='mixer', out_shape=jax.ShapeDtypeStruct...]
    unnamed x4 -> x1, local copies, waits for them, and re-layouts: 7.2 us -> 1.88 us
where the time goes in v1:
time: 47.9 us; the launch traced here: 47.8 us
  Pallas kernels  45.9 us (96%)
  local copies, waits for them, and re-layouts  1.88 us (4%)
    pallas_call x1, Pallas kernels, shards(): pl.pallas_call(mixer_kernel, name='mixer', out_shape=jax.ShapeDtypeStruct...  45.9 us
    unnamed x1, local copies, waits for them, and re-layouts  1.88 us

profile of v1, /device:TPU:33, one launch (start us, length us, event | category | flops | bytes accessed | tf_op | source)
XLA Modules:
  0.0 47.8 jit_solution(11093398687313963851)
XLA Ops:
  0.0 45.9 %mixer.1 = bf16[2,64,2048]{2,1,0:T(8,128)(2,1)} custom-call(bf16[2,64,2048]{2,1,0:T(8,128)(2,1)} %x_hbm.1, bf16[2048,512]{1,0:T(8,128)(2,1)} %in_w_hbm.1, bf16[2048,512]{1,0:T(8,128)(2,1)} %gate_w_hbm.1, bf16[512,2048]{1,0:T(8,128)(2,1)} %out_w_hbm.1, f32[1,2048]{1,0:T(1,128)} %bitcast.18, f32[32,64]{1,0:T(8,128)} %rate_re_hbm.1, f32[32,64]{1,0:T(8,128)} %rate_im_hbm.1, ...), custom_call_target="tpu_custom_call" | custom-call | tf_op jit(solution)/shard_map/mixer/pallas_call | solution.py:610
  45.9 1.9 %copy.17 = bf16[2,64,2048]{2,1,0:T(8,128)(2,1)} copy(bf16[2,64,2048]{2,1,0:T(8,128)(2,1)} %mixer.1) | data formatting | bytes 1048576

commit v2 on v1

--- a/solution.py
+++ b/solution.py
@@ -94,12 +94,12 @@
     read_im_hbm,
     skip_hbm,
     offset_hbm,
-    gain_hbm,
-    out_ref,
+    near_ref,
+    far_ref,
+    far_w_ref,
     tokens,
     in_w,
     gate_w,
-    out_w,
     norm_gain_ref,
     rate_re_ref,
     rate_im_ref,
@@ -110,8 +110,8 @@
     read_im_ref,
     skip_ref,
     offset_ref,
-    gain_ref,
     normed,
+    scales,
     raw_in,
     raw_gate,
     inputs,
@@ -142,8 +142,6 @@
     carry_x,
     lam_pack,
     act,
-    act_in,
-    near_sum,
     load_sem,
     x_send,
     x_recv,
@@ -198,8 +196,6 @@
                 (read_re_hbm, read_re_ref),
                 (read_im_hbm, read_im_ref),
                 (skip_hbm, skip_ref),
-                (gain_hbm, gain_ref),
-                (out_w_hbm, out_w.at[tp]),
             )
         )
     ]
@@ -264,31 +260,24 @@
                 row = s * blocks + b
                 log_pack[k, row : row + 1, :] = total[:, lo : lo + LANES]
 
-    pl.semaphore_wait(barrier, nx + nz - 1)
-    x_copy = remote(x_hbm, tokens.at[:, mine, :], x_send, x_recv, partner)
-    x_copy.start()
-    log_sends = to_x(log_pack, log_x, lx_send, lx_recv)
-    for copy in log_sends:
-        copy.start()
-    log_x[pl.ds(mx, 1)] = log_pack[pl.ds(mx, 1)]
-
     def norm(side):
-        per = own // 16
+        per = own // 32
 
         @pl.loop(0, sequences * per)
         def _(i):
             s = i // per
-            row = pl.multiple_of(side * own + (i % per) * 16, 16)
-            wide = tokens[s, pl.ds(row, 16), :].astype(F32)
+            row = pl.multiple_of(side * own + (i % per) * 32, 32)
+            wide = tokens[s, pl.ds(row, 32), :].astype(F32)
+            at = pl.ds(pl.multiple_of(i * 32, 32), 32)
+            normed[side, at, :] = (wide * norm_gain_ref[...]).astype(BF16)
             scale = lax.rsqrt(jnp.mean(wide * wide, axis=-1, keepdims=True) + EPS)
-            at = pl.ds(pl.multiple_of(i * 16, 16), 16)
-            normed[side, at, :] = (wide * scale * norm_gain_ref[...]).astype(BF16)
+            scales[side, at, :] = jnp.broadcast_to(scale, (32, 256))
 
     def project(side, weight, out):
         @pl.loop(0, width // 256)
         def _(c):
             lanes = pl.ds(pl.multiple_of(c * 256, 256), 256)
-            product = dot(normed[side], weight[:, lanes])
+            product = dot(normed[side], weight[:, lanes]) * scales[side]
             at = pl.ds(pl.multiple_of(side * own, own), own)
             out[:, at, lanes] = product.reshape(sequences, own, 256).astype(BF16)
 
@@ -346,6 +335,14 @@
     block_diagonal(wide_re, lambda g, at: two_re[at])
     block_diagonal(wide_im, lambda g, at: two_im[at])
 
+    pl.semaphore_wait(barrier, nx + nz - 1)
+    x_copy = remote(x_hbm, tokens.at[:, mine, :], x_send, x_recv, partner)
+    x_copy.start()
+    log_sends = to_x(log_pack, log_x, lx_send, lx_recv)
+    for copy in log_sends:
+        copy.start()
+    log_x[pl.ds(mx, 1)] = log_pack[pl.ds(mx, 1)]
+
     x_copy.wait()
     norm(1 - tp)
     project(1 - tp, in_w, raw_in)
@@ -355,6 +352,12 @@
         use, lanes = slice(h * hw, (h + 1) * hw), slice(h * half, (h + 1) * half)
         drive_re[:, lanes] = dot(inputs[:, use], wide_re[use, :])
         drive_im[:, lanes] = dot(inputs[:, use], wide_im[use, :])
+
+    for copy in log_sends:
+        copy.wait()
+    log_row[...] = jnp.sum(log_x[...], axis=0)
+    log_z_sends = to_z(log_row, log_z, lz_send, lz_recv)
+    start_z(log_z_sends)
 
     span = 512
 
@@ -371,10 +374,10 @@
 
             def body(t, now):
                 re, im = now
-                at = pl.ds(pl.multiple_of(t * 16, 16), 16)
+                at = pl.ds(pl.multiple_of(t * 4 * CHUNKS, 4 * CHUNKS), 4 * CHUNKS)
                 m, dr, di = mags[at, lanes], drive_re[at, lanes], drive_im[at, lanes]
                 kept = []
-                for u in range(2):
+                for u in range(4):
                     use = slice(u * CHUNKS, (u + 1) * CHUNKS)
                     ar, ai = m[use] * lr, m[use] * li
                     re, im = ar * re - ai * im + dr[use], ar * im + ai * re + di[use]
@@ -384,7 +387,7 @@
                     states_im[at, lanes] = jnp.concatenate([k[1] for k in kept], axis=0).astype(BF16)
                 return re, im
 
-            re, im = lax.fori_loop(0, steps // 2, body, start)
+            re, im = lax.fori_loop(0, steps // 4, body, start)
             if not keep:
                 ends[0, :, lanes] = re
                 ends[1, :, lanes] = im
@@ -421,11 +424,6 @@
         copy.start()
     sum_x[pl.ds(mx, 1)] = sum_pack[pl.ds(mx, 1)]
 
-    for copy in log_sends:
-        copy.wait()
-    log_row[...] = jnp.sum(log_x[...], axis=0)
-    log_z_sends = to_z(log_row, log_z, lz_send, lz_recv)
-    start_z(log_z_sends)
     for c in range(2):
         for blk in range(blocks):
             lanes = pl.ds(pl.multiple_of(mx * part + blk * LANES, LANES), LANES)
@@ -463,6 +461,28 @@
 
     loads[9].wait()
     project(tp, gate_w, raw_gate)
+    project(1 - tp, gate_w, raw_gate)
+    gates = dot(scan_order(rows), raw_gate[...].reshape(rows, width))
+    opened[...] = 1.0 / (1.0 + jnp.exp(-gates))
+
+    for copy in loads[10:13]:
+        copy.wait()
+    two_re, two_im = doubled(read_re_ref[...]), doubled(read_im_ref[...])
+
+    def coef(g):
+        lo = g // per_tile * LANES
+        return vec[6:7, lo : lo + LANES], vec[7:8, lo : lo + LANES]
+
+    def lifted_re(g, at):
+        kr, ki = coef(g)
+        return two_re[at] * kr - two_im[at] * ki
+
+    def lifted_im(g, at):
+        kr, ki = coef(g)
+        return -(two_re[at] * ki + two_im[at] * kr)
+
+    block_diagonal(lift_re, lifted_re)
+    block_diagonal(lift_im, lifted_im)
 
     for copy in sum_sends:
         copy.wait()
@@ -473,31 +493,8 @@
     sum_row[...] = jnp.concatenate(total, axis=0).astype(BF16)
     sum_z_sends = to_z(sum_row, sum_z, sz_send, sz_recv)
     start_z(sum_z_sends)
-    w_copy = remote(out_w_hbm, out_w.at[tp], w_send, w_recv, partner)
+    w_copy = remote(out_w_hbm, far_w_ref, w_send, w_recv, partner)
     w_copy.start()
-
-    project(1 - tp, gate_w, raw_gate)
-    gates = dot(scan_order(rows), raw_gate[...].reshape(rows, width))
-    opened[...] = 1.0 / (1.0 + jnp.exp(-gates))
-
-    for copy in loads[10:14]:
-        copy.wait()
-    two_re, two_im = doubled(read_re_ref[...]), doubled(read_im_ref[...])
-
-    def coef(g):
-        lo = g // per_tile * LANES
-        return vec[6:7, lo : lo + LANES], vec[7:8, lo : lo + LANES]
-
-    def lifted_re(g, at):
-        kr, ki = coef(g)
-        return two_re[at] * kr - two_im[at] * ki
-
-    def lifted_im(g, at):
-        kr, ki = coef(g)
-        return -(two_re[at] * ki + two_im[at] * kr)
-
-    block_diagonal(lift_re, lifted_re)
-    block_diagonal(lift_im, lifted_im)
 
     inside = [None] * nx
     inside[0] = (jnp.zeros((tile, LANES), F32), jnp.zeros((tile, LANES), F32))
@@ -549,27 +546,38 @@
     back = natural_order(rows)
     for h in range(2):
         act[:, :, h * hw : (h + 1) * hw] = dot(back, parts[h]).astype(BF16).reshape(sequences, 2 * own, hw)
-    a_copy = remote(act.at[:, theirs, :], act_in, a_send, a_recv, partner)
+    a_copy = remote(act.at[:, theirs, :], far_ref, a_send, a_recv, partner)
     a_copy.start()
-    near = act[:, mine, :].astype(F32).reshape(sequences * own, width)
-    near_square = jnp.sum(near * near, axis=-1, keepdims=True)
-    near = (near * gain_ref[:, pl.ds(pl.multiple_of(tp * width, width), width)]).astype(BF16)
-    loads[14].wait()
-    for c in range(depth // 256):
-        lanes = slice(c * 256, (c + 1) * 256)
-        near_sum[:, lanes] = dot(near, out_w[tp, :, lanes])
+    near_ref[...] = act[:, mine, :]
     w_copy.wait()
     a_copy.wait()
-    far = act_in[...].astype(F32).reshape(sequences * own, width)
-    scale = lax.rsqrt((near_square + jnp.sum(far * far, axis=-1, keepdims=True)) * (0.5 / width) + EPS)
-    far = (far * gain_ref[:, pl.ds(pl.multiple_of((1 - tp) * width, width), width)]).astype(BF16)
-    for c in range(depth // 256):
-        lanes = slice(c * 256, (c + 1) * 256)
-        result = (near_sum[:, lanes] + dot(far, out_w[1 - tp, :, lanes])) * scale
-        out_ref[:, :, lanes] = result.astype(BF16).reshape(sequences, own, 256)
 
     sent_z(log_z_sends)
     sent_z(sum_z_sends)
+
+
+def finish_kernel(near_ref, far_ref, gain_ref, near_w_ref, far_w_ref, out_hbm, staged, sem):
+    tp = lax.axis_index("tp")
+    sequences, own, width = near_ref.shape
+    depth = near_w_ref.shape[1]
+
+    def side(ref, which):
+        wide = ref[...].astype(F32).reshape(sequences * own, width)
+        gain = gain_ref[:, pl.ds(pl.multiple_of(which * width, width), width)]
+        return (wide * gain).astype(BF16), jnp.sum(wide * wide, axis=-1, keepdims=True)
+
+    near, near_square = side(near_ref, tp)
+    far, far_square = side(far_ref, 1 - tp)
+    scale = lax.rsqrt((near_square + far_square) * (0.5 / width) + EPS)
+    copies = []
+    for c in range(depth // 512):
+        lanes = slice(c * 512, (c + 1) * 512)
+        result = (dot(near, near_w_ref[:, lanes]) + dot(far, far_w_ref[:, lanes])) * scale
+        staged[:, :, lanes] = result.astype(BF16).reshape(sequences, own, 512)
+        copies.append(pltpu.make_async_copy(staged.at[:, :, lanes], out_hbm.at[:, :, lanes], sem.at[c]))
+        copies[-1].start()
+    for copy in copies:
+        copy.wait()
 
 
 def vmem():
@@ -607,17 +615,20 @@
     tile = sequences * (modes // nx // LANES)
     f32 = functools.partial(pltpu.VMEM, dtype=F32)
     b16 = functools.partial(pltpu.VMEM, dtype=BF16)
-    return pl.pallas_call(
+    near, far, far_w = pl.pallas_call(
         mixer_kernel,
         name="mixer",
-        out_shape=jax.ShapeDtypeStruct((sequences, own, depth), BF16),
-        in_specs=[hbm()] * 15,
-        out_specs=vmem(),
+        out_shape=[
+            pltpu.VMEM((sequences, own, width), BF16),
+            pltpu.VMEM((sequences, own, width), BF16),
+            pltpu.VMEM((width, depth), BF16),
+        ],
+        in_specs=[pl.BlockSpec(memory_space=pltpu.HBM)] * 14,
+        out_specs=[vmem()] * 3,
         scratch_shapes=[
             b16((sequences, 2 * own, depth)),
             b16((depth, width)),
             b16((depth, width)),
-            b16((2, width, depth)),
             f32((1, depth)),
             f32((groups, states)),
             f32((groups, states)),
@@ -628,8 +639,8 @@
             b16((width, states)),
             f32((1, width)),
             f32((sequences, groups, 2 * own)),
-            f32((1, 2 * width)),
             b16((2, sequences * own, depth)),
+            f32((2, sequences * own, 256)),
             b16((sequences, 2 * own, width)),
             b16((sequences, 2 * own, width)),
             b16((rows, width)),
@@ -660,9 +671,7 @@
             b16((nx, 2 * tile, LANES)),
             f32((2, tile, LANES)),
             b16((sequences, 2 * own, width)),
-            b16((sequences, own, width)),
-            f32((sequences * own, depth)),
-            dma((15,)),
+            dma((13,)),
             dma,
             dma,
             dma,
@@ -680,7 +689,7 @@
             dma,
             dma,
         ],
-        compiler_params=pltpu.CompilerParams(collective_id=0, has_side_effects=True),
+        compiler_params=pltpu.CompilerParams(collective_id=0, has_side_effects=True, vmem_limit_bytes=60 << 20),
     )(
         layer_input,
         in_weight,
@@ -696,8 +705,16 @@
         output_imag.reshape(width, states),
         skip_weight[None],
         jnp.swapaxes(decay_offset, 1, 2),
-        channel_gain[None],
     )
+    return pl.pallas_call(
+        finish_kernel,
+        name="finish",
+        out_shape=jax.ShapeDtypeStruct((sequences, own, depth), BF16),
+        in_specs=[vmem()] * 5,
+        out_specs=hbm(),
+        scratch_shapes=[b16((sequences, own, depth)), dma((depth // 512,))],
+        compiler_params=pltpu.CompilerParams(vmem_limit_bytes=16 << 20),
+    )(near, far, channel_gain[None], out_weight, far_w)
 
 
 def solution(mesh):

time: 47.9 us -> 44.8 us (0.935)
  Pallas kernels: 45.9 us -> 43 us
    pallas_call x1 -> x2, Pallas kernels: 45.9 us -> 43 us  [the longest x1 41.6 us: shards(): pl.pallas_call(mixer_kernel, name='mixer', out_shape=[pltpu.VMEM((sequenc...]
    unnamed x1 -> x4, local copies, waits for them, and re-layouts: 1.88 us -> 1.59 us
where the time goes in v2:
time: 44.8 us; the launch traced here: 44.6 us
  Pallas kernels  43 us (96%)
  local copies, waits for them, and re-layouts  1.59 us (4%)
    pallas_call x1, Pallas kernels, shards(): pl.pallas_call(mixer_kernel, name='mixer', out_shape=[pltpu.VMEM((sequenc...  41.6 us
    unnamed x4, local copies, waits for them, and re-layouts  1.59 us
    pallas_call x1, Pallas kernels, shards(): pl.pallas_call(finish_kernel, name='finish', out_shape=jax.ShapeDtypeStru...  1.42 us

profile of v2, /device:TPU:33, one launch (start us, length us, event | category | flops | bytes accessed | tf_op | source)
XLA Modules:
  0.0 44.6 jit_solution(11033264151135791567)
XLA Ops:
  0.0 0.0 copy-start.1
  0.0 41.6 %mixer.1 = (bf16[2,64,512]{2,1,0:T(8,128)(2,1)S(1)}, bf16[2,64,512]{2,1,0:T(8,128)(2,1)S(1)}, bf16[512,2048]{1,0:T(8,128)(2,1)S(1)}) custom-call(bf16[2,64,2048]{2,1,0:T(8,128)(2,1)} %x_hbm.1, bf16[2048,512]{1,0:T(8,128)(2,1)} %in_w_hbm.1, bf16[2048,512]{1,0:T(8,128)(2,1)} %gate_w_hbm.1, bf16[512,2048]{1,0:T(8,128)(2,1)} %near_w_ref.1, f32[1,2048]{1,0:T(1,128)} %bitcast.19, ...), custom_call_target="tpu_custom_call" | custom-call | tf_op jit(solution)/shard_map/mixer/pallas_call | solution.py:618
  41.6 0.0 copy-done.1
  41.6 0.0 copy-start
  41.6 1.6 %copy-done = bf16[512,2048]{1,0:T(8,128)(2,1)S(1)} copy-done((bf16[512,2048]{1,0:T(8,128)(2,1)S(1)}, bf16[512,2048]{1,0:T(8,128)(2,1)}, u32[]{:S(2)}) %copy-start) | copy-done | bytes 2097176
  43.2 1.4 %finish.1 = bf16[2,64,2048]{2,1,0:T(8,128)(2,1)} custom-call(bf16[2,64,512]{2,1,0:T(8,128)(2,1)S(1)} %get-tuple-element.8.near_ref, bf16[2,64,512]{2,1,0:T(8,128)(2,1)S(1)} %get-tuple-element.9.far_ref, f32[1,1024]{1,0:T(1,128)S(1)} %bitcast.13, bf16[512,2048]{1,0:T(8,128)(2,1)S(1)} %copy-done, bf16[512,2048]{1,0:T(8,128)(2,1)S(1)} %get-tuple-element.10.far_w_ref), custom_call_target="tpu_custom_call" | custom-call | tf_op jit(solution)/shard_map/finish/pallas_call | solution.py:709
Async XLA Ops:
  0.0 41.6 %copy-start.1 = (f32[1024]{0:T(1024)S(1)}, f32[1024]{0:T(1024)}, u32[]{:S(2)}) copy-start(f32[1024]{0:T(1024)} %param.28) | copy-start | bytes 12292
  41.6 1.6 %copy-start = (bf16[512,2048]{1,0:T(8,128)(2,1)S(1)}, bf16[512,2048]{1,0:T(8,128)(2,1)}, u32[]{:S(2)}) copy-start(bf16[512,2048]{1,0:T(8,128)(2,1)} %near_w_ref.1) | copy-start | bytes 6291460

commit v3 on v2

--- a/solution.py
+++ b/solution.py
@@ -94,7 +94,9 @@
     read_im_hbm,
     skip_hbm,
     offset_hbm,
+    gain_hbm,
     near_ref,
+    square_ref,
     far_ref,
     far_w_ref,
     tokens,
@@ -110,6 +112,8 @@
     read_im_ref,
     skip_ref,
     offset_ref,
+    gain_ref,
+    out_w,
     normed,
     scales,
     raw_in,
@@ -196,6 +200,8 @@
                 (read_re_hbm, read_re_ref),
                 (read_im_hbm, read_im_ref),
                 (skip_hbm, skip_ref),
+                (gain_hbm, gain_ref),
+                (out_w_hbm, out_w),
             )
         )
     ]
@@ -261,17 +267,13 @@
                 log_pack[k, row : row + 1, :] = total[:, lo : lo + LANES]
 
     def norm(side):
-        per = own // 32
-
-        @pl.loop(0, sequences * per)
-        def _(i):
-            s = i // per
-            row = pl.multiple_of(side * own + (i % per) * 32, 32)
-            wide = tokens[s, pl.ds(row, 32), :].astype(F32)
-            at = pl.ds(pl.multiple_of(i * 32, 32), 32)
-            normed[side, at, :] = (wide * norm_gain_ref[...]).astype(BF16)
-            scale = lax.rsqrt(jnp.mean(wide * wide, axis=-1, keepdims=True) + EPS)
-            scales[side, at, :] = jnp.broadcast_to(scale, (32, 256))
+        for s in range(sequences):
+            for r in range(0, own, 32):
+                wide = tokens[s, pl.ds(pl.multiple_of(side * own + r, 32), 32), :].astype(F32)
+                at = slice(s * own + r, s * own + r + 32)
+                normed[side, at, :] = (wide * norm_gain_ref[...]).astype(BF16)
+                scale = lax.rsqrt(jnp.mean(wide * wide, axis=-1, keepdims=True) + EPS)
+                scales[side, at, :] = jnp.broadcast_to(scale, (32, 256))
 
     def project(side, weight, out):
         @pl.loop(0, width // 256)
@@ -285,6 +287,14 @@
     norm(tp)
     loads[8].wait()
     project(tp, in_w, raw_in)
+
+    pl.semaphore_wait(barrier, nx + nz - 1)
+    log_sends = to_x(log_pack, log_x, lx_send, lx_recv)
+    for copy in log_sends:
+        copy.start()
+    x_copy = remote(tokens.at[:, mine, :], tokens.at[:, mine, :], x_send, x_recv, partner)
+    x_copy.start()
+    log_x[pl.ds(mx, 1)] = log_pack[pl.ds(mx, 1)]
 
     on_group = (iota((groups, modes), 1) >> 6) == iota((groups, modes), 0)
     rates = exact_dot(jnp.concatenate([rate_re_ref[...], rate_im_ref[...]], axis=0), spread_p)
@@ -335,15 +345,12 @@
     block_diagonal(wide_re, lambda g, at: two_re[at])
     block_diagonal(wide_im, lambda g, at: two_im[at])
 
-    pl.semaphore_wait(barrier, nx + nz - 1)
-    x_copy = remote(x_hbm, tokens.at[:, mine, :], x_send, x_recv, partner)
-    x_copy.start()
-    log_sends = to_x(log_pack, log_x, lx_send, lx_recv)
-    for copy in log_sends:
-        copy.start()
-    log_x[pl.ds(mx, 1)] = log_pack[pl.ds(mx, 1)]
-
     x_copy.wait()
+    w_copies = [
+        remote(out_w_hbm.at[at], far_w_ref.at[at], w_send.at[i], w_recv.at[i], partner)
+        for i, at in enumerate((pl.ds(0, hw), pl.ds(hw, hw)))
+    ]
+    w_copies[0].start()
     norm(1 - tp)
     project(1 - tp, in_w, raw_in)
     inputs[...] = dot(order, raw_in[...].reshape(rows, width)).astype(BF16)
@@ -352,12 +359,6 @@
         use, lanes = slice(h * hw, (h + 1) * hw), slice(h * half, (h + 1) * half)
         drive_re[:, lanes] = dot(inputs[:, use], wide_re[use, :])
         drive_im[:, lanes] = dot(inputs[:, use], wide_im[use, :])
-
-    for copy in log_sends:
-        copy.wait()
-    log_row[...] = jnp.sum(log_x[...], axis=0)
-    log_z_sends = to_z(log_row, log_z, lz_send, lz_recv)
-    start_z(log_z_sends)
 
     span = 512
 
@@ -424,6 +425,11 @@
         copy.start()
     sum_x[pl.ds(mx, 1)] = sum_pack[pl.ds(mx, 1)]
 
+    for copy in log_sends:
+        copy.wait()
+    log_row[...] = jnp.sum(log_x[...], axis=0)
+    log_z_sends = to_z(log_row, log_z, lz_send, lz_recv)
+    start_z(log_z_sends)
     for c in range(2):
         for blk in range(blocks):
             lanes = pl.ds(pl.multiple_of(mx * part + blk * LANES, LANES), LANES)
@@ -465,7 +471,7 @@
     gates = dot(scan_order(rows), raw_gate[...].reshape(rows, width))
     opened[...] = 1.0 / (1.0 + jnp.exp(-gates))
 
-    for copy in loads[10:13]:
+    for copy in loads[10:14]:
         copy.wait()
     two_re, two_im = doubled(read_re_ref[...]), doubled(read_im_ref[...])
 
@@ -493,8 +499,6 @@
     sum_row[...] = jnp.concatenate(total, axis=0).astype(BF16)
     sum_z_sends = to_z(sum_row, sum_z, sz_send, sz_recv)
     start_z(sum_z_sends)
-    w_copy = remote(out_w_hbm, far_w_ref, w_send, w_recv, partner)
-    w_copy.start()
 
     inside = [None] * nx
     inside[0] = (jnp.zeros((tile, LANES), F32), jnp.zeros((tile, LANES), F32))
@@ -533,6 +537,7 @@
             init[0, :, lanes] = before[2, :, lanes] + moved[0]
             init[1, :, lanes] = before[3, :, lanes] + moved[1]
 
+    w_copies[1].start()
     scan(init, True)
 
     parts = []
@@ -548,31 +553,34 @@
         act[:, :, h * hw : (h + 1) * hw] = dot(back, parts[h]).astype(BF16).reshape(sequences, 2 * own, hw)
     a_copy = remote(act.at[:, theirs, :], far_ref, a_send, a_recv, partner)
     a_copy.start()
-    near_ref[...] = act[:, mine, :]
-    w_copy.wait()
+    near = act[:, mine, :].astype(F32).reshape(sequences * own, width)
+    square_ref[...] = jnp.broadcast_to(jnp.sum(near * near, axis=-1, keepdims=True), square_ref.shape)
+    near = (near * gain_ref[:, pl.ds(pl.multiple_of(tp * width, width), width)]).astype(BF16)
+    loads[14].wait()
+    for c in range(depth // 512):
+        lanes = slice(c * 512, (c + 1) * 512)
+        near_ref[:, lanes] = dot(near, out_w[:, lanes])
+    for copy in w_copies:
+        copy.wait()
     a_copy.wait()
 
     sent_z(log_z_sends)
     sent_z(sum_z_sends)
 
 
-def finish_kernel(near_ref, far_ref, gain_ref, near_w_ref, far_w_ref, out_hbm, staged, sem):
+def finish_kernel(near_ref, square_ref, far_ref, gain_ref, far_w_ref, out_hbm, staged, sem):
     tp = lax.axis_index("tp")
-    sequences, own, width = near_ref.shape
-    depth = near_w_ref.shape[1]
-
-    def side(ref, which):
-        wide = ref[...].astype(F32).reshape(sequences * own, width)
-        gain = gain_ref[:, pl.ds(pl.multiple_of(which * width, width), width)]
-        return (wide * gain).astype(BF16), jnp.sum(wide * wide, axis=-1, keepdims=True)
-
-    near, near_square = side(near_ref, tp)
-    far, far_square = side(far_ref, 1 - tp)
-    scale = lax.rsqrt((near_square + far_square) * (0.5 / width) + EPS)
+    sequences, own, width = far_ref.shape
+    depth = far_w_ref.shape[1]
+
+    far = far_ref[...].astype(F32).reshape(sequences * own, width)
+    square = square_ref[:, :1] + jnp.sum(far * far, axis=-1, keepdims=True)
+    scale = lax.rsqrt(square * (0.5 / width) + EPS)
+    far = (far * gain_ref[:, pl.ds(pl.multiple_of((1 - tp) * width, width), width)]).astype(BF16)
     copies = []
     for c in range(depth // 512):
         lanes = slice(c * 512, (c + 1) * 512)
-        result = (dot(near, near_w_ref[:, lanes]) + dot(far, far_w_ref[:, lanes])) * scale
+        result = (near_ref[:, lanes] + dot(far, far_w_ref[:, lanes])) * scale
         staged[:, :, lanes] = result.astype(BF16).reshape(sequences, own, 512)
         copies.append(pltpu.make_async_copy(staged.at[:, :, lanes], out_hbm.at[:, :, lanes], sem.at[c]))
         copies[-1].start()
@@ -615,16 +623,17 @@
     tile = sequences * (modes // nx // LANES)
     f32 = functools.partial(pltpu.VMEM, dtype=F32)
     b16 = functools.partial(pltpu.VMEM, dtype=BF16)
-    near, far, far_w = pl.pallas_call(
+    near, square, far, far_w = pl.pallas_call(
         mixer_kernel,
         name="mixer",
         out_shape=[
-            pltpu.VMEM((sequences, own, width), BF16),
+            pltpu.VMEM((sequences * own, depth), F32),
+            pltpu.VMEM((sequences * own, LANES), F32),
             pltpu.VMEM((sequences, own, width), BF16),
             pltpu.VMEM((width, depth), BF16),
         ],
-        in_specs=[pl.BlockSpec(memory_space=pltpu.HBM)] * 14,
-        out_specs=[vmem()] * 3,
+        in_specs=[pl.BlockSpec(memory_space=pltpu.HBM)] * 15,
+        out_specs=[vmem()] * 4,
         scratch_shapes=[
             b16((sequences, 2 * own, depth)),
             b16((depth, width)),
@@ -639,6 +648,8 @@
             b16((width, states)),
             f32((1, width)),
             f32((sequences, groups, 2 * own)),
+            f32((1, 2 * width)),
+            b16((width, depth)),
             b16((2, sequences * own, depth)),
             f32((2, sequences * own, 256)),
             b16((sequences, 2 * own, width)),
@@ -671,11 +682,11 @@
             b16((nx, 2 * tile, LANES)),
             f32((2, tile, LANES)),
             b16((sequences, 2 * own, width)),
-            dma((13,)),
+            dma((15,)),
             dma,
             dma,
-            dma,
-            dma,
+            dma((2,)),
+            dma((2,)),
             dma((nx - 1,)),
             dma((nx - 1,)),
             dma((nz - 1,)),
@@ -689,7 +700,7 @@
             dma,
             dma,
         ],
-        compiler_params=pltpu.CompilerParams(collective_id=0, has_side_effects=True, vmem_limit_bytes=60 << 20),
+        compiler_params=pltpu.CompilerParams(collective_id=0, has_side_effects=True, vmem_limit_bytes=67043328 - (5 << 20)),
     )(
         layer_input,
         in_weight,
@@ -705,6 +716,7 @@
         output_imag.reshape(width, states),
         skip_weight[None],
         jnp.swapaxes(decay_offset, 1, 2),
+        channel_gain[None],
     )
     return pl.pallas_call(
         finish_kernel,
@@ -714,7 +726,7 @@
         out_specs=hbm(),
         scratch_shapes=[b16((sequences, own, depth)), dma((depth // 512,))],
         compiler_params=pltpu.CompilerParams(vmem_limit_bytes=16 << 20),
-    )(near, far, channel_gain[None], out_weight, far_w)
+    )(near, square, far, channel_gain[None], far_w)
 
 
 def solution(mesh):

time: 44.8 us -> 42 us (0.938)
  local copies, waits for them, and re-layouts: 1.59 us -> 0.01 us
  Pallas kernels: 43 us -> 41.9 us
    unnamed x4 -> x2, local copies, waits for them, and re-layouts: 1.59 us -> 0.01 us
    pallas_call x1, Pallas kernels: 41.6 us -> 40.7 us  [shards(): pl.pallas_call(mixer_kernel, name='mixer', out_shape=[pltpu.VMEM((sequenc...]
where the time goes in v3:
time: 42 us; the launch traced here: 41.9 us
  Pallas kernels  41.9 us (100%)
    pallas_call x1, Pallas kernels, shards(): pl.pallas_call(mixer_kernel, name='mixer', out_shape=[pltpu.VMEM((sequenc...  40.7 us
    pallas_call x1, Pallas kernels, shards(): pl.pallas_call(finish_kernel, name='finish', out_shape=jax.ShapeDtypeStru...  1.17 us

profile of v3, /device:TPU:33, one launch (start us, length us, event | category | flops | bytes accessed | tf_op | source)
XLA Modules:
  0.0 41.9 jit_solution(5701427892794228248)
XLA Ops:
  0.0 0.0 copy-start
  0.0 40.7 %mixer.1 = (f32[128,2048]{1,0:T(8,128)S(1)}, f32[128,128]{1,0:T(8,128)S(1)}, bf16[2,64,512]{2,1,0:T(8,128)(2,1)S(1)}, bf16[512,2048]{1,0:T(8,128)(2,1)S(1)}) custom-call(bf16[2,64,2048]{2,1,0:T(8,128)(2,1)} %x_hbm.1, bf16[2048,512]{1,0:T(8,128)(2,1)} %in_w_hbm.1, bf16[2048,512]{1,0:T(8,128)(2,1)} %gate_w_hbm.1, bf16[512,2048]{1,0:T(8,128)(2,1)} %out_w_hbm.1, ...), custom_call_target="tpu_custom_call" | custom-call | tf_op jit(solution)/shard_map/mixer/pallas_call | solution.py:626
  40.8 0.0 copy-done
  40.8 1.2 %finish.1 = bf16[2,64,2048]{2,1,0:T(8,128)(2,1)} custom-call(f32[128,2048]{1,0:T(8,128)S(1)} %get-tuple-element.9.near_ref, f32[128,128]{1,0:T(8,128)S(1)} %get-tuple-element.10.square_ref, bf16[2,64,512]{2,1,0:T(8,128)(2,1)S(1)} %get-tuple-element.11.far_ref, f32[1,1024]{1,0:T(1,128)S(1)} %bitcast.14, bf16[512,2048]{1,0:T(8,128)(2,1)S(1)} %get-tuple-element.12.far_w_ref), custom_call_target="tpu_custom_call" | custom-call | tf_op jit(solution)/shard_map/finish/pallas_call | solution.py:721
Async XLA Ops:
  0.0 40.8 %copy-start = (f32[1024]{0:T(1024)S(1)}, f32[1024]{0:T(1024)}, u32[]{:S(2)}) copy-start(f32[1024]{0:T(1024)} %param.28) | copy-start | bytes 12292

commit v4 on v3

--- a/solution.py
+++ b/solution.py
@@ -17,6 +17,7 @@
 EPS = 1e-06
 LANES = 128
 CHUNKS = 8
+BLOCK = 4
 
 
 def dot(a, b):
@@ -137,11 +138,15 @@
     log_x,
     log_row,
     log_z,
+    log_block,
+    log_far,
     sum_stage,
     sum_pack,
     sum_x,
     sum_row,
     sum_z,
+    sum_block,
+    sum_far,
     carry_pack,
     carry_x,
     lam_pack,
@@ -155,10 +160,14 @@
     lx_recv,
     lz_send,
     lz_recv,
+    lf_send,
+    lf_recv,
     sx_send,
     sx_recv,
     sz_send,
     sz_recv,
+    sf_send,
+    sf_recv,
     cx_send,
     cx_recv,
     a_send,
@@ -208,15 +217,23 @@
     for copy in loads:
         copy.start()
 
-    log_z[...] = jnp.zeros_like(log_z)
-    sum_z[...] = jnp.zeros_like(sum_z)
+    for ref in (log_z, sum_z, log_far, sum_far):
+        ref[...] = jnp.zeros_like(ref)
     barrier = pltpu.get_barrier_semaphore()
     pl.semaphore_signal(barrier, inc=1, device_id=partner, device_id_type=MESH)
     for d in range(1, nx):
         pl.semaphore_signal(barrier, inc=1, device_id={"sp_1": lax.rem(mx + d, nx)}, device_id_type=MESH)
-    far_first = sorted(range(1, nz), key=lambda d: -min(d, nz - d))
-    for d in far_first:
-        pl.semaphore_signal(barrier, inc=1, device_id={"sp_0": lax.rem(mz + d, nz)}, device_id_type=MESH)
+    count = nz // BLOCK
+    block, place_z = mz // BLOCK, mz % BLOCK
+    ends_block = place_z == BLOCK - 1
+
+    def signal_z(z):
+        pl.semaphore_signal(barrier, inc=1, device_id={"sp_0": z}, device_id_type=MESH)
+
+    for d in range(1, BLOCK):
+        pl.when(d <= place_z)(lambda d=d: signal_z(mz - d))
+    for e in range(1, count):
+        pl.when(e <= block)(lambda e=e: signal_z((block - e) * BLOCK + BLOCK - 1))
 
     def remote(source, target, send, recv, device):
         return pltpu.make_async_remote_copy(
@@ -230,23 +247,46 @@
             made.append(remote(source.at[k], target.at[mx], send.at[d - 1], recv.at[d - 1], {"sp_1": k}))
         return made
 
-    def to_z(source, target, send, recv):
+    def to_block(source, target, send, recv):
         return {
             d: remote(source, target.at[d - 1], send.at[d - 1], recv.at[d - 1], {"sp_0": lax.rem(mz + d, nz)})
-            for d in far_first
+            for d in range(1, BLOCK)
         }
 
-    def start_z(made):
+    def to_later(source, target, send, recv):
+        made = {}
+        for d in sorted(range(1, nz - BLOCK + 1), key=lambda d: -min(d, nz - d)):
+            e = (d + BLOCK - 1) // BLOCK - 1
+            made[d] = remote(source, target.at[e], send.at[d - 1], recv.at[e], {"sp_0": lax.rem(mz + d, nz)})
+        return made
+
+    def start_block(made):
         for d, copy in made.items():
-            pl.when(mz + d < nz)(copy.start)
-
-    def recv_z(made):
+            pl.when(place_z + d < BLOCK)(copy.start)
+
+    def start_later(made):
+        @pl.when(ends_block)
+        def _():
+            for d, copy in made.items():
+                pl.when(mz + d < nz)(copy.start)
+
+    def recv_block(made):
         for d, copy in made.items():
-            pl.when(d <= mz)(copy.wait_recv)
-
-    def sent_z(made):
+            pl.when(d <= place_z)(copy.wait_recv)
+
+    def recv_later(made):
+        for e in range(1, count):
+            pl.when(e <= block)(made[(e - 1) * BLOCK + 1].wait_recv)
+
+    def sent_block(made):
         for d, copy in made.items():
-            pl.when(mz + d < nz)(copy.wait_send)
+            pl.when(place_z + d < BLOCK)(copy.wait_send)
+
+    def sent_later(made):
+        @pl.when(ends_block)
+        def _():
+            for d, copy in made.items():
+                pl.when(mz + d < nz)(copy.wait_send)
 
     for copy in loads[1:6]:
         copy.wait()
@@ -288,7 +328,8 @@
     loads[8].wait()
     project(tp, in_w, raw_in)
 
-    pl.semaphore_wait(barrier, nx + nz - 1)
+    later = jnp.where(ends_block, nz - 1 - mz, 0)
+    pl.semaphore_wait(barrier, nx + BLOCK - 1 - place_z + later)
     log_sends = to_x(log_pack, log_x, lx_send, lx_recv)
     for copy in log_sends:
         copy.start()
@@ -428,8 +469,8 @@
     for copy in log_sends:
         copy.wait()
     log_row[...] = jnp.sum(log_x[...], axis=0)
-    log_z_sends = to_z(log_row, log_z, lz_send, lz_recv)
-    start_z(log_z_sends)
+    log_z_sends = to_block(log_row, log_z, lz_send, lz_recv)
+    start_block(log_z_sends)
     for c in range(2):
         for blk in range(blocks):
             lanes = pl.ds(pl.multiple_of(mx * part + blk * LANES, LANES), LANES)
@@ -497,25 +538,46 @@
     for k in range(1, nx):
         total = plus(total, cmul(to_end[k], came[k]))
     sum_row[...] = jnp.concatenate(total, axis=0).astype(BF16)
-    sum_z_sends = to_z(sum_row, sum_z, sz_send, sz_recv)
-    start_z(sum_z_sends)
+    sum_z_sends = to_block(sum_row, sum_z, sz_send, sz_recv)
+    start_block(sum_z_sends)
 
     inside = [None] * nx
     inside[0] = (jnp.zeros((tile, LANES), F32), jnp.zeros((tile, LANES), F32))
     for k in range(1, nx):
         inside[k] = plus(cmul(inside[k - 1], grow(logs[k - 1], lam_dev)), came[k - 1])
-    recv_z(log_z_sends)
-    weights = {}
-    gone, power = jnp.zeros((tile, LANES), F32), one
-    for d in range(1, nz):
+    recv_block(log_z_sends)
+    zero = jnp.zeros((tile, LANES), F32)
+    gone, power, weights = zero, one, {}
+    for d in range(1, BLOCK):
         weights[d] = grow(gone, power)
         gone = gone + log_z[d - 1]
-        power = cmul(power, lam_pow[nx])
-
-    recv_z(sum_z_sends)
-    carry = inside[0]
-    for d in range(1, nz):
+        power = tuple(jnp.where(d <= place_z, n, o) for n, o in zip(cmul(power, lam_pow[nx]), power))
+    through = grow(gone, power)
+    log_block[...] = gone + jnp.sum(log_x[...], axis=0)
+    log_far_sends = to_later(log_block, log_far, lf_send, lf_recv)
+    start_later(log_far_sends)
+    lam_block = one
+    for _ in range(BLOCK):
+        lam_block = cmul(lam_block, lam_pow[nx])
+
+    recv_block(sum_z_sends)
+    carry = (zero, zero)
+    for d in range(1, BLOCK):
         carry = plus(carry, cmul(weights[d], halves(sum_z[d - 1])))
+    filled = plus(cmul(carry, grow(jnp.sum(log_x[...], axis=0), lam_pow[nx])), total)
+    sum_block[...] = jnp.concatenate(filled, axis=0).astype(BF16)
+    sum_far_sends = to_later(sum_block, sum_far, sf_send, sf_recv)
+    start_later(sum_far_sends)
+
+    recv_later(log_far_sends)
+    gone, power = zero, one
+    for e in range(1, count):
+        weights[e] = cmul(through, grow(gone, power))
+        gone = gone + log_far[e - 1]
+        power = cmul(power, lam_block)
+    recv_later(sum_far_sends)
+    for e in range(1, count):
+        carry = plus(carry, cmul(weights[e], halves(sum_far[e - 1])))
     for k in range(nx):
         carry_pack[k] = jnp.concatenate(plus(cmul(carry, to_start[k]), inside[k]), axis=0).astype(BF16)
     carry_sends = to_x(carry_pack, carry_x, cx_send, cx_recv)
@@ -564,8 +626,10 @@
         copy.wait()
     a_copy.wait()
 
-    sent_z(log_z_sends)
-    sent_z(sum_z_sends)
+    sent_block(log_z_sends)
+    sent_block(sum_z_sends)
+    sent_later(log_far_sends)
+    sent_later(sum_far_sends)
 
 
 def finish_kernel(near_ref, square_ref, far_ref, gain_ref, far_w_ref, out_hbm, staged, sem):
@@ -620,6 +684,7 @@
     modes = groups * states
     rows = sequences * 2 * own
     dma = pltpu.SemaphoreType.DMA
+    later = nz // BLOCK - 1
     tile = sequences * (modes // nx // LANES)
     f32 = functools.partial(pltpu.VMEM, dtype=F32)
     b16 = functools.partial(pltpu.VMEM, dtype=BF16)
@@ -672,12 +737,16 @@
             f32((nx, tile, LANES)),
             f32((nx, tile, LANES)),
             f32((tile, LANES)),
-            f32((nz - 1, tile, LANES)),
+            f32((BLOCK - 1, tile, LANES)),
+            f32((tile, LANES)),
+            f32((later, tile, LANES)),
             f32((nx, 2 * tile, LANES)),
             b16((nx, 2 * tile, LANES)),
             b16((nx, 2 * tile, LANES)),
             b16((2 * tile, LANES)),
-            b16((nz - 1, 2 * tile, LANES)),
+            b16((BLOCK - 1, 2 * tile, LANES)),
+            b16((2 * tile, LANES)),
+            b16((later, 2 * tile, LANES)),
             b16((nx, 2 * tile, LANES)),
             b16((nx, 2 * tile, LANES)),
             f32((2, tile, LANES)),
@@ -689,12 +758,16 @@
             dma((2,)),
             dma((nx - 1,)),
             dma((nx - 1,)),
-            dma((nz - 1,)),
-            dma((nz - 1,)),
+            dma((BLOCK - 1,)),
+            dma((BLOCK - 1,)),
+            dma((nz - BLOCK,)),
+            dma((later,)),
             dma((nx - 1,)),
             dma((nx - 1,)),
-            dma((nz - 1,)),
-            dma((nz - 1,)),
+            dma((BLOCK - 1,)),
+            dma((BLOCK - 1,)),
+            dma((nz - BLOCK,)),
+            dma((later,)),
             dma((nx - 1,)),
             dma((nx - 1,)),
             dma,

time: 42 us -> 39.3 us (0.936)
  Pallas kernels: 41.9 us -> 39.2 us
    pallas_call x1, Pallas kernels: 40.7 us -> 38 us  [shards(): pl.pallas_call(mixer_kernel, name='mixer', out_shape=[pltpu.VMEM((sequenc...]
where the time goes in v4:
time: 39.3 us; the launch traced here: 39.2 us
  Pallas kernels  39.2 us (100%)
    pallas_call x1, Pallas kernels, shards(): pl.pallas_call(mixer_kernel, name='mixer', out_shape=[pltpu.VMEM((sequenc...  38 us
    pallas_call x1, Pallas kernels, shards(): pl.pallas_call(finish_kernel, name='finish', out_shape=jax.ShapeDtypeStru...  1.16 us

profile of v4, /device:TPU:33, one launch (start us, length us, event | category | flops | bytes accessed | tf_op | source)
XLA Modules:
  0.0 39.2 jit_solution(6266352215301880151)
XLA Ops:
  0.0 0.0 copy-start
  0.0 38.0 %mixer.1 = (f32[128,2048]{1,0:T(8,128)S(1)}, f32[128,128]{1,0:T(8,128)S(1)}, bf16[2,64,512]{2,1,0:T(8,128)(2,1)S(1)}, bf16[512,2048]{1,0:T(8,128)(2,1)S(1)}) custom-call(bf16[2,64,2048]{2,1,0:T(8,128)(2,1)} %x_hbm.1, bf16[2048,512]{1,0:T(8,128)(2,1)} %in_w_hbm.1, bf16[2048,512]{1,0:T(8,128)(2,1)} %gate_w_hbm.1, bf16[512,2048]{1,0:T(8,128)(2,1)} %out_w_hbm.1, ...), custom_call_target="tpu_custom_call" | custom-call | tf_op jit(solution)/shard_map/mixer/pallas_call | solution.py:691
  38.0 0.0 copy-done
  38.0 1.2 %finish.1 = bf16[2,64,2048]{2,1,0:T(8,128)(2,1)} custom-call(f32[128,2048]{1,0:T(8,128)S(1)} %get-tuple-element.9.near_ref, f32[128,128]{1,0:T(8,128)S(1)} %get-tuple-element.10.square_ref, bf16[2,64,512]{2,1,0:T(8,128)(2,1)S(1)} %get-tuple-element.11.far_ref, f32[1,1024]{1,0:T(1,128)S(1)} %bitcast.14, bf16[512,2048]{1,0:T(8,128)(2,1)S(1)} %get-tuple-element.12.far_w_ref), custom_call_target="tpu_custom_call" | custom-call | tf_op jit(solution)/shard_map/finish/pallas_call | solution.py:794
Async XLA Ops:
  0.0 38.0 %copy-start = (f32[1024]{0:T(1024)S(1)}, f32[1024]{0:T(1024)}, u32[]{:S(2)}) copy-start(f32[1024]{0:T(1024)} %param.28) | copy-start | bytes 12292

commit v5 on v4

--- a/solution.py
+++ b/solution.py
@@ -18,6 +18,7 @@
 LANES = 128
 CHUNKS = 8
 BLOCK = 4
+UNROLL = 8
 
 
 def dot(a, b):
@@ -122,6 +123,8 @@
     inputs,
     opened,
     mags,
+    trans_re,
+    trans_im,
     wide_re,
     wide_im,
     drive_re,
@@ -147,8 +150,6 @@
     sum_z,
     sum_block,
     sum_far,
-    carry_pack,
-    carry_x,
     lam_pack,
     act,
     load_sem,
@@ -168,8 +169,6 @@
     sz_recv,
     sf_send,
     sf_recv,
-    cx_send,
-    cx_recv,
     a_send,
     a_recv,
 ):
@@ -183,9 +182,10 @@
     modes = groups * states
     steps = rows // CHUNKS
     quarters = CHUNKS // sequences
-    part = modes // nx
-    blocks = part // LANES
-    tile = sequences * blocks
+    tile = CHUNKS
+    blocks = tile // sequences
+    part = blocks * LANES
+    packs = modes // part
     half = modes // 2
     hw = width // 2
     mine = pl.ds(pl.multiple_of(tp * own, own), own)
@@ -242,9 +242,9 @@
 
     def to_x(source, target, send, recv):
         made = []
-        for d in range(1, nx):
+        for d in sorted(range(1, nx), key=lambda d: -min(d, nx - d)):
             k = lax.rem(mx + d, nx)
-            made.append(remote(source.at[k], target.at[mx], send.at[d - 1], recv.at[d - 1], {"sp_1": k}))
+            made.append(remote(source, target.at[mx], send.at[d - 1], recv.at[d - 1], {"sp_1": k}))
         return made
 
     def to_block(source, target, send, recv):
@@ -255,7 +255,7 @@
 
     def to_later(source, target, send, recv):
         made = {}
-        for d in sorted(range(1, nz - BLOCK + 1), key=lambda d: -min(d, nz - d)):
+        for d in sorted(range(1, nz - BLOCK + 1), key=lambda d: min(d, nz - d)):
             e = (d + BLOCK - 1) // BLOCK - 1
             made[d] = remote(source, target.at[e], send.at[d - 1], recv.at[e], {"sp_0": lax.rem(mz + d, nz)})
         return made
@@ -287,6 +287,9 @@
         def _():
             for d, copy in made.items():
                 pl.when(mz + d < nz)(copy.wait_send)
+
+    for ref in (wide_re, wide_im, lift_re, lift_im):
+        ref[...] = jnp.zeros_like(ref)
 
     for copy in loads[1:6]:
         copy.wait()
@@ -300,7 +303,7 @@
     vec[pl.ds(16, CHUNKS), :] = chunk_logs
     for s in range(sequences):
         total = jnp.sum(chunk_logs[s * quarters : (s + 1) * quarters], axis=0, keepdims=True)
-        for k in range(nx):
+        for k in range(packs):
             for b in range(blocks):
                 lo = k * part + b * LANES
                 row = s * blocks + b
@@ -323,19 +326,16 @@
             at = pl.ds(pl.multiple_of(side * own, own), own)
             out[:, at, lanes] = product.reshape(sequences, own, 256).astype(BF16)
 
+    later = jnp.where(ends_block, nz - 1 - mz, 0)
     loads[0].wait()
-    norm(tp)
-    loads[8].wait()
-    project(tp, in_w, raw_in)
-
-    later = jnp.where(ends_block, nz - 1 - mz, 0)
     pl.semaphore_wait(barrier, nx + BLOCK - 1 - place_z + later)
     log_sends = to_x(log_pack, log_x, lx_send, lx_recv)
     for copy in log_sends:
         copy.start()
     x_copy = remote(tokens.at[:, mine, :], tokens.at[:, mine, :], x_send, x_recv, partner)
     x_copy.start()
-    log_x[pl.ds(mx, 1)] = log_pack[pl.ds(mx, 1)]
+    log_x[mx] = log_pack[...]
+    norm(tp)
 
     on_group = (iota((groups, modes), 1) >> 6) == iota((groups, modes), 0)
     rates = exact_dot(jnp.concatenate([rate_re_ref[...], rate_im_ref[...]], axis=0), spread_p)
@@ -373,7 +373,6 @@
     on_lane = iota((channels, LANES), 1) // states
 
     def block_diagonal(target, value):
-        target[...] = jnp.zeros_like(target)
         for g in range(groups):
             at = slice(g * channels, (g + 1) * channels)
             lo = (g % (groups // 2)) // per_tile * LANES
@@ -386,10 +385,13 @@
     block_diagonal(wide_re, lambda g, at: two_re[at])
     block_diagonal(wide_im, lambda g, at: two_im[at])
 
+    loads[8].wait()
+    project(tp, in_w, raw_in)
+
     x_copy.wait()
     w_copies = [
         remote(out_w_hbm.at[at], far_w_ref.at[at], w_send.at[i], w_recv.at[i], partner)
-        for i, at in enumerate((pl.ds(0, hw), pl.ds(hw, hw)))
+        for i, at in enumerate((pl.ds(0, 3 * width // 4), pl.ds(3 * width // 4, width // 4)))
     ]
     w_copies[0].start()
     norm(1 - tp)
@@ -407,8 +409,8 @@
         @pl.loop(0, modes // span)
         def _(c):
             lanes = pl.ds(pl.multiple_of(c * span, span), span)
-            lr = jnp.broadcast_to(vec[0:1, lanes], (CHUNKS, span))
-            li = jnp.broadcast_to(vec[1:2, lanes], (CHUNKS, span))
+            lr = jnp.broadcast_to(vec[0:1, lanes], (UNROLL * CHUNKS, span))
+            li = jnp.broadcast_to(vec[1:2, lanes], (UNROLL * CHUNKS, span))
             if first is None:
                 start = (jnp.zeros((CHUNKS, span), F32), jnp.zeros((CHUNKS, span), F32))
             else:
@@ -416,20 +418,29 @@
 
             def body(t, now):
                 re, im = now
-                at = pl.ds(pl.multiple_of(t * 4 * CHUNKS, 4 * CHUNKS), 4 * CHUNKS)
-                m, dr, di = mags[at, lanes], drive_re[at, lanes], drive_im[at, lanes]
+                at = pl.ds(pl.multiple_of(t * UNROLL * CHUNKS, UNROLL * CHUNKS), UNROLL * CHUNKS)
+                dr, di = drive_re[at, lanes], drive_im[at, lanes]
+                if keep:
+                    ar, ai = trans_re[at, lanes], trans_im[at, lanes]
+                else:
+                    m = mags[at, lanes]
+                    ar, ai = m * lr, m * li
+                    trans_re[at, lanes] = ar
+                    trans_im[at, lanes] = ai
                 kept = []
-                for u in range(4):
+                for u in range(UNROLL):
                     use = slice(u * CHUNKS, (u + 1) * CHUNKS)
-                    ar, ai = m[use] * lr, m[use] * li
-                    re, im = ar * re - ai * im + dr[use], ar * im + ai * re + di[use]
+                    re, im = (
+                        ar[use] * re - ai[use] * im + dr[use],
+                        ar[use] * im + ai[use] * re + di[use],
+                    )
                     kept.append((re, im))
                 if keep:
                     states_re[at, lanes] = jnp.concatenate([k[0] for k in kept], axis=0).astype(BF16)
                     states_im[at, lanes] = jnp.concatenate([k[1] for k in kept], axis=0).astype(BF16)
                 return re, im
 
-            re, im = lax.fori_loop(0, steps // 4, body, start)
+            re, im = lax.fori_loop(0, steps // UNROLL, body, start)
             if not keep:
                 ends[0, :, lanes] = re
                 ends[1, :, lanes] = im
@@ -453,7 +464,7 @@
     for c in range(2):
         for s in range(sequences):
             last = (s + 1) * quarters - 1
-            for k in range(nx):
+            for k in range(packs):
                 for blk in range(blocks):
                     lo = k * part + blk * LANES
                     row = c * tile + s * blocks + blk
@@ -464,7 +475,7 @@
     sum_sends = to_x(sum_pack, sum_x, sx_send, sx_recv)
     for copy in sum_sends:
         copy.start()
-    sum_x[pl.ds(mx, 1)] = sum_pack[pl.ds(mx, 1)]
+    sum_x[mx] = sum_pack[...]
 
     for copy in log_sends:
         copy.wait()
@@ -472,14 +483,15 @@
     log_z_sends = to_block(log_row, log_z, lz_send, lz_recv)
     start_block(log_z_sends)
     for c in range(2):
-        for blk in range(blocks):
-            lanes = pl.ds(pl.multiple_of(mx * part + blk * LANES, LANES), LANES)
-            value = vec[4 + c : 5 + c, lanes]
-            for s in range(sequences):
-                row = s * blocks + blk
-                lam_pack[c, row : row + 1, :] = value
+        for k in range(packs):
+            for blk in range(blocks):
+                lo = k * part + blk * LANES
+                for s in range(sequences):
+                    row = s * blocks + blk
+                    lam_pack[c, k, row : row + 1, :] = vec[4 + c : 5 + c, lo : lo + LANES]
     lam_dev = (lam_pack[0], lam_pack[1])
-    one = (jnp.ones((tile, LANES), F32), jnp.zeros((tile, LANES), F32))
+    zero = jnp.zeros((packs, tile, LANES), F32)
+    one = (jnp.ones((packs, tile, LANES), F32), zero)
     lam_pow = [one]
     for _ in range(nx):
         lam_pow.append(cmul(lam_pow[-1], lam_dev))
@@ -490,21 +502,23 @@
 
     def halves(value):
         wide = value.astype(F32)
-        return wide[:tile], wide[tile:]
+        return wide[:, :tile], wide[:, tile:]
 
     def plus(u, v):
         return u[0] + v[0], u[1] + v[1]
 
     logs = [log_x[k] for k in range(nx)]
-    to_end, to_start = [None] * nx, [None] * nx
-    gone = jnp.zeros((tile, LANES), F32)
+    to_end = [None] * nx
+    gone = zero
     for k in range(nx - 1, -1, -1):
         to_end[k] = grow(gone, lam_pow[nx - 1 - k])
         gone = gone + logs[k]
-    gone = jnp.zeros((tile, LANES), F32)
-    for k in range(nx):
-        to_start[k] = grow(gone, lam_pow[k])
-        gone = gone + logs[k]
+    row_logs = gone
+    gone, power = zero, one
+    for k in range(nx - 1):
+        gone = jnp.where(k < mx, gone + logs[k], gone)
+        power = tuple(jnp.where(k < mx, n, o) for n, o in zip(lam_pow[k + 1], power))
+    to_own = grow(gone, power)
 
     loads[9].wait()
     project(tp, gate_w, raw_gate)
@@ -530,6 +544,20 @@
 
     block_diagonal(lift_re, lifted_re)
     block_diagonal(lift_im, lifted_im)
+
+    recv_block(log_z_sends)
+    gone, power, weights = zero, one, {}
+    for d in range(1, BLOCK):
+        weights[d] = grow(gone, power)
+        gone = gone + log_z[d - 1]
+        power = tuple(jnp.where(d <= place_z, n, o) for n, o in zip(cmul(power, lam_pow[nx]), power))
+    through = grow(gone, power)
+    log_block[...] = gone + row_logs
+    log_far_sends = to_later(log_block, log_far, lf_send, lf_recv)
+    start_later(log_far_sends)
+    lam_block = one
+    for _ in range(BLOCK):
+        lam_block = cmul(lam_block, lam_pow[nx])
 
     for copy in sum_sends:
         copy.wait()
@@ -537,35 +565,20 @@
     total = cmul(to_end[0], came[0])
     for k in range(1, nx):
         total = plus(total, cmul(to_end[k], came[k]))
-    sum_row[...] = jnp.concatenate(total, axis=0).astype(BF16)
+    sum_row[...] = jnp.concatenate(total, axis=1).astype(BF16)
     sum_z_sends = to_block(sum_row, sum_z, sz_send, sz_recv)
     start_block(sum_z_sends)
 
-    inside = [None] * nx
-    inside[0] = (jnp.zeros((tile, LANES), F32), jnp.zeros((tile, LANES), F32))
-    for k in range(1, nx):
-        inside[k] = plus(cmul(inside[k - 1], grow(logs[k - 1], lam_dev)), came[k - 1])
-    recv_block(log_z_sends)
-    zero = jnp.zeros((tile, LANES), F32)
-    gone, power, weights = zero, one, {}
-    for d in range(1, BLOCK):
-        weights[d] = grow(gone, power)
-        gone = gone + log_z[d - 1]
-        power = tuple(jnp.where(d <= place_z, n, o) for n, o in zip(cmul(power, lam_pow[nx]), power))
-    through = grow(gone, power)
-    log_block[...] = gone + jnp.sum(log_x[...], axis=0)
-    log_far_sends = to_later(log_block, log_far, lf_send, lf_recv)
-    start_later(log_far_sends)
-    lam_block = one
-    for _ in range(BLOCK):
-        lam_block = cmul(lam_block, lam_pow[nx])
-
+    inside = (zero, zero)
+    for k in range(nx - 1):
+        new = plus(cmul(inside, grow(logs[k], lam_dev)), came[k])
+        inside = tuple(jnp.where(k < mx, n, o) for n, o in zip(new, inside))
     recv_block(sum_z_sends)
     carry = (zero, zero)
     for d in range(1, BLOCK):
         carry = plus(carry, cmul(weights[d], halves(sum_z[d - 1])))
-    filled = plus(cmul(carry, grow(jnp.sum(log_x[...], axis=0), lam_pow[nx])), total)
-    sum_block[...] = jnp.concatenate(filled, axis=0).astype(BF16)
+    filled = plus(cmul(carry, grow(row_logs, lam_pow[nx])), total)
+    sum_block[...] = jnp.concatenate(filled, axis=1).astype(BF16)
     sum_far_sends = to_later(sum_block, sum_far, sf_send, sf_recv)
     start_later(sum_far_sends)
 
@@ -578,22 +591,14 @@
     recv_later(sum_far_sends)
     for e in range(1, count):
         carry = plus(carry, cmul(weights[e], halves(sum_far[e - 1])))
-    for k in range(nx):
-        carry_pack[k] = jnp.concatenate(plus(cmul(carry, to_start[k]), inside[k]), axis=0).astype(BF16)
-    carry_sends = to_x(carry_pack, carry_x, cx_send, cx_recv)
-    for copy in carry_sends:
-        copy.start()
-    carry_x[pl.ds(mx, 1)] = carry_pack[pl.ds(mx, 1)]
-    for copy in carry_sends:
-        copy.wait()
+    carry = plus(cmul(carry, to_own), inside)
     upper = iota((CHUNKS, LANES), 0) < quarters
-    for k in range(nx):
-        got = carry_x[k].astype(F32)
+    for k in range(packs):
         for blk in range(blocks):
             lo = k * part + blk * LANES
             lanes = slice(lo, lo + LANES)
             into = tuple(
-                jnp.where(upper, got[c * tile + blk][None], got[c * tile + blocks + blk][None]) for c in range(2)
+                jnp.where(upper, v[k, blk : blk + 1, :], v[k, blocks + blk : blocks + blk + 1, :]) for v in carry
             )
             moved = cmul((before[0, :, lanes], before[1, :, lanes]), into)
             init[0, :, lanes] = before[2, :, lanes] + moved[0]
@@ -685,7 +690,8 @@
     rows = sequences * 2 * own
     dma = pltpu.SemaphoreType.DMA
     later = nz // BLOCK - 1
-    tile = sequences * (modes // nx // LANES)
+    tile = CHUNKS
+    packs = modes // (tile // sequences * LANES)
     f32 = functools.partial(pltpu.VMEM, dtype=F32)
     b16 = functools.partial(pltpu.VMEM, dtype=BF16)
     near, square, far, far_w = pl.pallas_call(
@@ -722,6 +728,8 @@
             b16((rows, width)),
             f32((rows, width)),
             f32((rows, modes)),
+            f32((rows, modes)),
+            f32((rows, modes)),
             b16((width, modes // 2)),
             b16((width, modes // 2)),
             f32((rows, modes)),
@@ -734,22 +742,20 @@
             f32((2, CHUNKS, modes)),
             f32((4, CHUNKS, modes)),
             f32((2, CHUNKS, modes)),
-            f32((nx, tile, LANES)),
-            f32((nx, tile, LANES)),
-            f32((tile, LANES)),
-            f32((BLOCK - 1, tile, LANES)),
-            f32((tile, LANES)),
-            f32((later, tile, LANES)),
-            f32((nx, 2 * tile, LANES)),
-            b16((nx, 2 * tile, LANES)),
-            b16((nx, 2 * tile, LANES)),
-            b16((2 * tile, LANES)),
-            b16((BLOCK - 1, 2 * tile, LANES)),
-            b16((2 * tile, LANES)),
-            b16((later, 2 * tile, LANES)),
-            b16((nx, 2 * tile, LANES)),
-            b16((nx, 2 * tile, LANES)),
-            f32((2, tile, LANES)),
+            f32((packs, tile, LANES)),
+            f32((nx, packs, tile, LANES)),
+            f32((packs, tile, LANES)),
+            f32((BLOCK - 1, packs, tile, LANES)),
+            f32((packs, tile, LANES)),
+            f32((later, packs, tile, LANES)),
+            f32((packs, 2 * tile, LANES)),
+            b16((packs, 2 * tile, LANES)),
+            b16((nx, packs, 2 * tile, LANES)),
+            b16((packs, 2 * tile, LANES)),
+            b16((BLOCK - 1, packs, 2 * tile, LANES)),
+            b16((packs, 2 * tile, LANES)),
+            b16((later, packs, 2 * tile, LANES)),
+            f32((2, packs, tile, LANES)),
             b16((sequences, 2 * own, width)),
             dma((15,)),
             dma,
@@ -768,8 +774,6 @@
             dma((BLOCK - 1,)),
             dma((nz - BLOCK,)),
             dma((later,)),
-            dma((nx - 1,)),
-            dma((nx - 1,)),
             dma,
             dma,
         ],

time: 39.3 us -> 35.4 us (0.901)
  Pallas kernels: 39.2 us -> 35.3 us
    pallas_call x1, Pallas kernels: 38 us -> 34.1 us  [shards(): pl.pallas_call(mixer_kernel, name='mixer', out_shape=[pltpu.VMEM((sequenc...]
where the time goes in v5:
time: 35.4 us; the launch traced here: 35.3 us
  Pallas kernels  35.3 us (100%)
    pallas_call x1, Pallas kernels, shards(): pl.pallas_call(mixer_kernel, name='mixer', out_shape=[pltpu.VMEM((sequenc...  34.1 us
    pallas_call x1, Pallas kernels, shards(): pl.pallas_call(finish_kernel, name='finish', out_shape=jax.ShapeDtypeStru...  1.17 us

profile of v5, /device:TPU:33, one launch (start us, length us, event | category | flops | bytes accessed | tf_op | source)
XLA Modules:
  0.0 35.3 jit_solution(9129400766312684584)
XLA Ops:
  0.0 0.0 copy-start
  0.0 34.1 %mixer.1 = (f32[128,2048]{1,0:T(8,128)S(1)}, f32[128,128]{1,0:T(8,128)S(1)}, bf16[2,64,512]{2,1,0:T(8,128)(2,1)S(1)}, bf16[512,2048]{1,0:T(8,128)(2,1)S(1)}) custom-call(bf16[2,64,2048]{2,1,0:T(8,128)(2,1)} %x_hbm.1, bf16[2048,512]{1,0:T(8,128)(2,1)} %in_w_hbm.1, bf16[2048,512]{1,0:T(8,128)(2,1)} %gate_w_hbm.1, bf16[512,2048]{1,0:T(8,128)(2,1)} %out_w_hbm.1, ...), custom_call_target="tpu_custom_call" | custom-call | tf_op jit(solution)/shard_map/mixer/pallas_call | solution.py:697
  34.1 0.0 copy-done
  34.1 1.2 %finish.1 = bf16[2,64,2048]{2,1,0:T(8,128)(2,1)} custom-call(f32[128,2048]{1,0:T(8,128)S(1)} %get-tuple-element.9.near_ref, f32[128,128]{1,0:T(8,128)S(1)} %get-tuple-element.10.square_ref, bf16[2,64,512]{2,1,0:T(8,128)(2,1)S(1)} %get-tuple-element.11.far_ref, f32[1,1024]{1,0:T(1,128)S(1)} %bitcast.14, bf16[512,2048]{1,0:T(8,128)(2,1)S(1)} %get-tuple-element.12.far_w_ref), custom_call_target="tpu_custom_call" | custom-call | tf_op jit(solution)/shard_map/finish/pallas_call | solution.py:798
Async XLA Ops:
  0.0 34.1 %copy-start = (f32[1024]{0:T(1024)S(1)}, f32[1024]{0:T(1024)}, u32[]{:S(2)}) copy-start(f32[1024]{0:T(1024)} %param.28) | copy-start | bytes 12292

commit v6 on v5

--- a/solution.py
+++ b/solution.py
@@ -328,6 +328,25 @@
 
     later = jnp.where(ends_block, nz - 1 - mz, 0)
     loads[0].wait()
+    norm(tp)
+
+    on_group = (iota((groups, modes), 1) >> 6) == iota((groups, modes), 0)
+    rates = exact_dot(jnp.concatenate([rate_re_ref[...], rate_im_ref[...]], axis=0), spread_p)
+    rate_re = jnp.sum(jnp.where(on_group, rates[:groups], 0.0), axis=0, keepdims=True)
+    rate_im = jnp.sum(jnp.where(on_group, rates[groups:], 0.0), axis=0, keepdims=True)
+    real_step, angle = rate_re * step, rate_im * step
+    size = jnp.exp(real_step)
+    cosine, sine = small_cosine(angle), small_sine(angle)
+    lam = (size * cosine, size * sine)
+    power = lam
+    for _ in range(int(math.log2(steps))):
+        power = cmul(power, power)
+    lam_chunk = power
+    for _ in range(int(math.log2(quarters))):
+        power = cmul(power, power)
+    for i, value in enumerate((*lam, *lam_chunk, *power, rate_re, rate_im, real_step, angle)):
+        vec[i : i + 1, :] = value
+
     pl.semaphore_wait(barrier, nx + BLOCK - 1 - place_z + later)
     log_sends = to_x(log_pack, log_x, lx_send, lx_recv)
     for copy in log_sends:
@@ -335,30 +354,6 @@
     x_copy = remote(tokens.at[:, mine, :], tokens.at[:, mine, :], x_send, x_recv, partner)
     x_copy.start()
     log_x[mx] = log_pack[...]
-    norm(tp)
-
-    on_group = (iota((groups, modes), 1) >> 6) == iota((groups, modes), 0)
-    rates = exact_dot(jnp.concatenate([rate_re_ref[...], rate_im_ref[...]], axis=0), spread_p)
-    rate_re = jnp.sum(jnp.where(on_group, rates[:groups], 0.0), axis=0, keepdims=True)
-    rate_im = jnp.sum(jnp.where(on_group, rates[groups:], 0.0), axis=0, keepdims=True)
-    real_step, angle = rate_re * step, rate_im * step
-    size = jnp.exp(real_step)
-    cosine, sine = small_cosine(angle), small_sine(angle)
-    half_sine = small_sine(0.5 * angle)
-    top_re = small_expm1(real_step) * cosine - 2.0 * half_sine * half_sine
-    top_im = size * sine
-    inverse = 1.0 / (rate_re * rate_re + rate_im * rate_im)
-    coef_re = (top_re * rate_re + top_im * rate_im) * inverse
-    coef_im = (top_im * rate_re - top_re * rate_im) * inverse
-    lam = (size * cosine, size * sine)
-    power = lam
-    for _ in range(int(math.log2(steps))):
-        power = cmul(power, power)
-    lam_chunk = power
-    for _ in range(int(math.log2(quarters))):
-        power = cmul(power, power)
-    for i, value in enumerate((*lam, *lam_chunk, *power, coef_re, coef_im)):
-        vec[i : i + 1, :] = value
 
     order = scan_order(rows)
     pieces = [dot(order, piece) for piece in split(jnp.exp(offsets))]
@@ -530,9 +525,17 @@
         copy.wait()
     two_re, two_im = doubled(read_re_ref[...]), doubled(read_im_ref[...])
 
+    rate_re, rate_im, real_step, angle = (vec[i : i + 1, :] for i in range(6, 10))
+    half_sine = small_sine(0.5 * angle)
+    top_re = small_expm1(real_step) * small_cosine(angle) - 2.0 * half_sine * half_sine
+    top_im = jnp.exp(real_step) * small_sine(angle)
+    inverse = 1.0 / (rate_re * rate_re + rate_im * rate_im)
+    vec[10:11, :] = (top_re * rate_re + top_im * rate_im) * inverse
+    vec[11:12, :] = (top_im * rate_re - top_re * rate_im) * inverse
+
     def coef(g):
         lo = g // per_tile * LANES
-        return vec[6:7, lo : lo + LANES], vec[7:8, lo : lo + LANES]
+        return vec[10:11, lo : lo + LANES], vec[11:12, lo : lo + LANES]
 
     def lifted_re(g, at):
         kr, ki = coef(g)

time: 35.4 us -> 35.3 us (level)
  no operation moved by 1% of the time
where the time goes in v6:
time: 35.3 us; the launch traced here: 35.1 us
  Pallas kernels  35.1 us (99%)
    pallas_call x1, Pallas kernels, shards(): pl.pallas_call(mixer_kernel, name='mixer', out_shape=[pltpu.VMEM((sequenc...  34 us
    pallas_call x1, Pallas kernels, shards(): pl.pallas_call(finish_kernel, name='finish', out_shape=jax.ShapeDtypeStru...  1.17 us

profile of v6, /device:TPU:33, one launch (start us, length us, event | category | flops | bytes accessed | tf_op | source)
XLA Modules:
  0.0 35.1 jit_solution(13568142799273063273)
XLA Ops:
  0.0 0.0 copy-start
  0.0 34.0 %mixer.1 = (f32[128,2048]{1,0:T(8,128)S(1)}, f32[128,128]{1,0:T(8,128)S(1)}, bf16[2,64,512]{2,1,0:T(8,128)(2,1)S(1)}, bf16[512,2048]{1,0:T(8,128)(2,1)S(1)}) custom-call(bf16[2,64,2048]{2,1,0:T(8,128)(2,1)} %x_hbm.1, bf16[2048,512]{1,0:T(8,128)(2,1)} %in_w_hbm.1, bf16[2048,512]{1,0:T(8,128)(2,1)} %gate_w_hbm.1, bf16[512,2048]{1,0:T(8,128)(2,1)} %out_w_hbm.1, ...), custom_call_target="tpu_custom_call" | custom-call | tf_op jit(solution)/shard_map/mixer/pallas_call | solution.py:700
  34.0 0.0 copy-done
  34.0 1.2 %finish.1 = bf16[2,64,2048]{2,1,0:T(8,128)(2,1)} custom-call(f32[128,2048]{1,0:T(8,128)S(1)} %get-tuple-element.9.near_ref, f32[128,128]{1,0:T(8,128)S(1)} %get-tuple-element.10.square_ref, bf16[2,64,512]{2,1,0:T(8,128)(2,1)S(1)} %get-tuple-element.11.far_ref, f32[1,1024]{1,0:T(1,128)S(1)} %bitcast.14, bf16[512,2048]{1,0:T(8,128)(2,1)S(1)} %get-tuple-element.12.far_w_ref), custom_call_target="tpu_custom_call" | custom-call | tf_op jit(solution)/shard_map/finish/pallas_call | solution.py:801
Async XLA Ops:
  0.0 34.0 %copy-start = (f32[1024]{0:T(1024)S(1)}, f32[1024]{0:T(1024)}, u32[]{:S(2)}) copy-start(f32[1024]{0:T(1024)} %param.28) | copy-start | bytes 12292

commit v7 on v6

--- a/solution.py
+++ b/solution.py
@@ -330,6 +330,14 @@
     loads[0].wait()
     norm(tp)
 
+    pl.semaphore_wait(barrier, nx + BLOCK - 1 - place_z + later)
+    log_sends = to_x(log_pack, log_x, lx_send, lx_recv)
+    for copy in log_sends:
+        copy.start()
+    x_copy = remote(tokens.at[:, mine, :], tokens.at[:, mine, :], x_send, x_recv, partner)
+    x_copy.start()
+    log_x[mx] = log_pack[...]
+
     on_group = (iota((groups, modes), 1) >> 6) == iota((groups, modes), 0)
     rates = exact_dot(jnp.concatenate([rate_re_ref[...], rate_im_ref[...]], axis=0), spread_p)
     rate_re = jnp.sum(jnp.where(on_group, rates[:groups], 0.0), axis=0, keepdims=True)
@@ -346,14 +354,6 @@
         power = cmul(power, power)
     for i, value in enumerate((*lam, *lam_chunk, *power, rate_re, rate_im, real_step, angle)):
         vec[i : i + 1, :] = value
-
-    pl.semaphore_wait(barrier, nx + BLOCK - 1 - place_z + later)
-    log_sends = to_x(log_pack, log_x, lx_send, lx_recv)
-    for copy in log_sends:
-        copy.start()
-    x_copy = remote(tokens.at[:, mine, :], tokens.at[:, mine, :], x_send, x_recv, partner)
-    x_copy.start()
-    log_x[mx] = log_pack[...]
 
     order = scan_order(rows)
     pieces = [dot(order, piece) for piece in split(jnp.exp(offsets))]

time: 35.3 us -> 35.3 us (level)
  no operation moved by 1% of the time
where the time goes in v7:
time: 35.3 us; the launch traced here: 35.1 us
  Pallas kernels  35.1 us (99%)
    pallas_call x1, Pallas kernels, shards(): pl.pallas_call(mixer_kernel, name='mixer', out_shape=[pltpu.VMEM((sequenc...  34 us
    pallas_call x1, Pallas kernels, shards(): pl.pallas_call(finish_kernel, name='finish', out_shape=jax.ShapeDtypeStru...  1.17 us

profile of v7, /device:TPU:33, one launch (start us, length us, event | category | flops | bytes accessed | tf_op | source)
XLA Modules:
  0.0 35.1 jit_solution(11593377103925068688)
XLA Ops:
  0.0 0.0 copy-start
  0.0 34.0 %mixer.1 = (f32[128,2048]{1,0:T(8,128)S(1)}, f32[128,128]{1,0:T(8,128)S(1)}, bf16[2,64,512]{2,1,0:T(8,128)(2,1)S(1)}, bf16[512,2048]{1,0:T(8,128)(2,1)S(1)}) custom-call(bf16[2,64,2048]{2,1,0:T(8,128)(2,1)} %x_hbm.1, bf16[2048,512]{1,0:T(8,128)(2,1)} %in_w_hbm.1, bf16[2048,512]{1,0:T(8,128)(2,1)} %gate_w_hbm.1, bf16[512,2048]{1,0:T(8,128)(2,1)} %out_w_hbm.1, ...), custom_call_target="tpu_custom_call" | custom-call | tf_op jit(solution)/shard_map/mixer/pallas_call | solution.py:700
  34.0 0.0 copy-done
  34.0 1.2 %finish.1 = bf16[2,64,2048]{2,1,0:T(8,128)(2,1)} custom-call(f32[128,2048]{1,0:T(8,128)S(1)} %get-tuple-element.9.near_ref, f32[128,128]{1,0:T(8,128)S(1)} %get-tuple-element.10.square_ref, bf16[2,64,512]{2,1,0:T(8,128)(2,1)S(1)} %get-tuple-element.11.far_ref, f32[1,1024]{1,0:T(1,128)S(1)} %bitcast.14, bf16[512,2048]{1,0:T(8,128)(2,1)S(1)} %get-tuple-element.12.far_w_ref), custom_call_target="tpu_custom_call" | custom-call | tf_op jit(solution)/shard_map/finish/pallas_call | solution.py:801
Async XLA Ops:
  0.0 34.0 %copy-start = (f32[1024]{0:T(1024)S(1)}, f32[1024]{0:T(1024)}, u32[]{:S(2)}) copy-start(f32[1024]{0:T(1024)} %param.28) | copy-start | bytes 12292
